TPU v7x, 32 devices: a whole 2x2x4 slice. The times are simulated.
32 devices in a mesh: sp: 16 (over z, y, x), tp: 2 (over core).
Axes of the slice: x: 2, y: 2, z: 4, core: 2. Of those that a mesh axis runs over, the one named last changes fastest.
Arguments:
- stream: bfloat16 [4096, 2048], P(('sp', 'tp')), may hold values from -6 to 6
- outer_gate: bfloat16 [4096, 1024], P('sp', 'tp'), may hold values from -6 to 6
- inner_gate: bfloat16 [4096, 1024], P('sp', 'tp'), may hold values from -6 to 6
- conv_values: bfloat16 [4096, 1024], P('sp', 'tp'), may hold values from -6 to 6
- doc_ids: int32 [4096], P('sp'), may hold values from 0 to 7, never falling along the last dimension, each value on 1 to 1024 neighbouring positions
- conv_taps: float32 [3, 1024], P(None, 'tp'), may hold values from -3.5 to 3.5
- out_weight: bfloat16 [1024, 2048], replicated, may hold values from -0.1875 to 0.1875
- norm_gain: float32 [2048], replicated, may hold values from 0.1 to 1.9
- route_ids: int32 [4096, 2], P(('sp', 'tp')), may hold values from 0 to 31, all different within a row; in each aligned block of 128 rows (0 to 127, 128 to 255, ...) at most 16 rows name the same one
- route_logits: float32 [4096, 2], P(('sp', 'tp')), may hold values from -4 to 4
- group_weight: float32 [4096], P(('sp', 'tp')), may hold values from 0.25 to 1
- w_gate: bfloat16 [32, 2048, 1024], P(('sp', 'tp')), may hold values from -0.125 to 0.125
- w_up: bfloat16 [32, 2048, 1024], P(('sp', 'tp')), may hold values from -0.125 to 0.125
- w_down: bfloat16 [32, 1024, 2048], P(('sp', 'tp')), may hold values from -0.1875 to 0.1875
Outputs:
- result: bfloat16 [4096, 2048], P(('sp', 'tp'))
Inputs may be any that keep to these rules, and one draw needn't show every extreme that they name: `route_ids`: the two experts of a token differ. In the rows of one device (aligned blocks of 128 rows) no expert is named more than 16 times, a bound that some block reaches. `doc_ids`: document numbers never fall along the sequence; a document has 1 to 1024 positions and one has exactly 1024.
All inputs are finite; a program needn't handle non-finite values.
Results may differ from a plain program's by a relative error of at most 0.0052.
Values may be sent and summed in bfloat16 or wider, within the bound.
A program may use at most 64 MiB of HBM per device.

v0:
```python
import functools

import jax
import jax.numpy as jnp
from jax import lax
from jax.experimental import pallas as pl
from jax.experimental.pallas import tpu as pltpu
from jax.sharding import PartitionSpec as P


def padded_2(shard, sides, width):
    for axis, dim in sides:
        size, length = (lax.axis_size(axis), shard.shape[dim])
        up = [(i, (i + 1) % size) for i in range(size - 1)]
        down = [(j, i) for i, j in up]
        last = lax.slice_in_dim(shard, length - width, length, axis=dim)
        leading = lax.slice_in_dim(shard, 0, width, axis=dim)
        before = lax.ppermute(last, axis, up)
        after = lax.ppermute(leading, axis, down)
        shard = jnp.concatenate([before, shard, after], axis=dim)
    return shard


def on_device(
    stream,
    outer_gate,
    inner_gate,
    conv_values,
    doc_ids,
    conv_taps,
    out_weight,
    norm_gain,
    route_ids,
    route_logits,
    group_weight,
    w_gate,
    w_up,
    w_down,
):
    tok_rows = stream.shape[0]
    width = stream.shape[1]
    product = (inner_gate.astype(jnp.float32) * conv_values.astype(jnp.float32)).astype(
        jnp.bfloat16
    )
    doc_float = doc_ids.astype(jnp.bfloat16)
    padded, padded_docs = (padded_2(product, (("sp", 0),), 1), padded_2(doc_float, (("sp", 0),), 1))
    same_prev = (padded_docs[:-2] == doc_float).astype(jnp.float32)[:, None]
    same_next = (padded_docs[2:] == doc_float).astype(jnp.float32)[:, None]
    conv = (
        conv_taps[0] * padded[:-2].astype(jnp.float32) * same_prev
        + conv_taps[1] * product.astype(jnp.float32)
        + conv_taps[2] * padded[2:].astype(jnp.float32) * same_next
    )
    mixed = (outer_gate.astype(jnp.float32) * conv).astype(jnp.bfloat16)
    channels = lax.all_to_all(mixed, "tp", split_axis=0, concat_axis=1, tiled=True)
    projected = jnp.dot(channels, out_weight, preferred_element_type=jnp.float32)
    resid = stream.astype(jnp.float32) + projected
    scale = lax.rsqrt(jnp.mean(resid * resid, axis=-1, keepdims=True) + 1e-06)
    normed = (resid * scale * norm_gain).astype(jnp.bfloat16)
    expert_total = lax.axis_size("sp") * lax.axis_size("tp")
    top_count = route_ids.shape[1]
    capacity = 2 * tok_rows * top_count // expert_total
    flat_ids = route_ids.reshape(-1)
    one_hot = (flat_ids[:, None] == jnp.arange(expert_total, dtype=jnp.int32)[None, :]).astype(
        jnp.int32
    )
    rank = jnp.sum((jnp.cumsum(one_hot, axis=0) - 1) * one_hot, axis=1)
    slot = flat_ids * capacity + rank
    slot_count = expert_total * capacity
    source_row = (
        jnp.zeros((slot_count,), jnp.int32)
        .at[slot]
        .set(jnp.arange(flat_ids.shape[0], dtype=jnp.int32) // top_count)
    )
    filled = jnp.zeros((slot_count,), jnp.bool_).at[slot].set(True)
    outgoing = jnp.where(filled[:, None], normed[source_row], jnp.zeros((), jnp.bfloat16)).reshape(
        expert_total, capacity, width
    )
    arrived = lax.all_to_all(outgoing, ("sp", "tp"), split_axis=0, concat_axis=0, tiled=True)
    sources, items, features = arrived.shape
    rows_in = arrived.reshape(sources * items, features)
    hidden = (
        jax.nn.silu(jnp.dot(rows_in, w_gate[0], preferred_element_type=jnp.float32))
        * jnp.dot(rows_in, w_up[0], preferred_element_type=jnp.float32)
    ).astype(jnp.bfloat16)
    outputs = jnp.dot(hidden, w_down[0], preferred_element_type=jnp.float32).astype(jnp.bfloat16)
    returned = lax.all_to_all(
        outputs.reshape(sources, items, features),
        ("sp", "tp"),
        split_axis=0,
        concat_axis=0,
        tiled=True,
    )
    picked = (
        returned.reshape(slot_count, width)[slot]
        .astype(jnp.float32)
        .reshape(tok_rows, top_count, width)
    )
    expo = jnp.exp(route_logits)
    gate = group_weight[:, None] * expo / jnp.sum(expo, axis=1, keepdims=True)
    result = resid + jnp.sum(gate[:, :, None] * picked, axis=1)
    return result.astype(jnp.bfloat16)


MESH = pl.DeviceIdType.MESH
F32, BF16 = jnp.float32, jnp.bfloat16


def dot(a, b):
    return jnp.dot(a, b, preferred_element_type=F32)


PARTS = 4


def near(z, h):
    return 2 * (z // 2) + (z % 2 + h) % 2


def across(z):
    return 2 * ((z // 2 + 1) % 2) + z % 2


def fused_kernel(
    tp_size, planes, per_plane, cap,
    stream, outer, inner, values, docs, taps, gain, ids, logits, weight,
    ow_hbm, wg_hbm, wu_hbm, wd_hbm,
    out,
    ow, wg, wu, wd, edge_out, edge_in, doc_in, mix, mix_in, resid, normed, hidden,
    send, recv, outb, ret, far, far_ids, far_logits, far_weight, halves, part_in,
    load_sem, edge_send, edge_recv, mix_send, mix_recv, self_sem, self_back,
    out_sem, in_sem, back_sem, home_sem, far_send, far_recv, part_send, part_recv,
):
    sp, tp = lax.axis_index("sp"), lax.axis_index("tp")
    sp_size = planes * per_plane // tp_size
    total = planes * per_plane
    me = sp * tp_size + tp
    z, p = me // per_plane, me % per_plane
    rows, width = stream.shape
    chan = inner.shape[1]
    length = inner.shape[0]

    def place(index):
        return (index // tp_size, index % tp_size)

    loads = [
        pltpu.make_async_copy(src, dst, load_sem.at[i])
        for i, (src, dst) in enumerate(
            ((ow_hbm, ow), (wg_hbm.at[0], wg), (wu_hbm.at[0], wu), (wd_hbm.at[0], wd))
        )
    ]
    for load in loads:
        load.start()

    barrier = pltpu.get_barrier_semaphore()

    def greet(i, carry):
        pl.semaphore_signal(
            barrier, inc=1, device_id=place((me + i) % total), device_id_type=MESH
        )
        return carry

    lax.fori_loop(1, total, greet, 0)
    product = (inner[...].astype(F32) * values[...].astype(F32)).astype(BF16)
    edge_out[0] = product[:16]
    edge_out[1] = product[length - 16 :]
    pl.semaphore_wait(barrier, total - 1)

    left, right = ((sp + sp_size - 1) % sp_size, tp), ((sp + 1) % sp_size, tp)
    edges = []
    for side, (dest, src) in enumerate(((right, edge_out.at[1]), (left, edge_out.at[0]))):
        for kind, (source, target) in enumerate(
            ((src, edge_in.at[side]), (docs, doc_in.at[side]))
        ):
            edges.append(
                pltpu.make_async_remote_copy(
                    src_ref=source,
                    dst_ref=target,
                    send_sem=edge_send.at[2 * side + kind],
                    recv_sem=edge_recv.at[2 * side + kind],
                    device_id=dest,
                    device_id_type=MESH,
                )
            )
    for edge in edges:
        edge.start()

    mirror = place(across(z) * per_plane + p)

    def to_mirror(src, dst, source_sem, target_sem):
        return pltpu.make_async_remote_copy(
            src_ref=src,
            dst_ref=dst,
            send_sem=source_sem,
            recv_sem=target_sem,
            device_id=mirror,
            device_id_type=MESH,
        )

    routes = [
        to_mirror(src, dst, far_send.at[i], far_recv.at[i])
        for i, (src, dst) in enumerate(
            ((ids, far_ids), (logits, far_logits), (weight, far_weight))
        )
    ]
    for route in routes:
        route.start()

    top = ids.shape[0]

    def gate_columns(logit, group):
        expo = jnp.exp(logit[...])
        gates = group[...] * expo / jnp.sum(expo, axis=0, keepdims=True)
        return [
            jnp.transpose(jnp.broadcast_to(gates[k : k + 1], (rows, rows)))[:, :1]
            for k in range(top)
        ]

    before = (
        lax.broadcasted_iota(jnp.int32, (rows, rows), 0)
        < lax.broadcasted_iota(jnp.int32, (rows, rows), 1)
    ).astype(F32).astype(BF16)
    rank_of = lax.broadcasted_iota(jnp.int32, (per_plane, cap, rows), 1).astype(F32)

    def slots(plane, named_ids):
        id_rows = [named_ids[k : k + 1, :] for k in range(top)]
        expert = lax.broadcasted_iota(jnp.int32, (per_plane, rows), 0) + plane * per_plane
        hits = [(row == expert).astype(F32) for row in id_rows]
        named = sum(hits)
        ahead = dot(named.astype(BF16), before)

        def spread(hit):
            at = jnp.where(hit > 0, ahead, -1.0)
            grid = jnp.broadcast_to(at[:, None, :], (per_plane, cap, rows))
            return jnp.where(grid == rank_of, 1.0, 0.0).reshape(per_plane * cap, rows)

        return named, hits, spread

    for edge in edges:
        edge.wait()

    doc = jnp.broadcast_to(docs[...], (8, length))
    lane = lax.broadcasted_iota(jnp.int32, (8, length), 1)
    prior = jnp.where(
        lane == 0,
        pltpu.roll(jnp.broadcast_to(doc_in[0], (8, length)), 1, axis=1),
        pltpu.roll(doc, 1, axis=1),
    )
    later = jnp.where(
        lane == length - 1,
        pltpu.roll(jnp.broadcast_to(doc_in[1], (8, length)), length - 1, axis=1),
        pltpu.roll(doc, length - 1, axis=1),
    )
    spot = lane + sp * length
    same_prev = jnp.where((prior == doc) & (spot > 0), 1.0, 0.0)
    same_next = jnp.where((later == doc) & (spot < sp_size * length - 1), 1.0, 0.0)

    def column(row):
        return jnp.transpose(jnp.broadcast_to(row[:1], (128, length)))[:, :1]

    prod = product.astype(F32)
    row_at = lax.broadcasted_iota(jnp.int32, (length, chan), 0)
    prev = jnp.where(row_at == 0, edge_in[0].astype(F32)[15:16], pltpu.roll(prod, 1, axis=0))
    nxt = jnp.where(
        row_at == length - 1,
        edge_in[1].astype(F32)[:1],
        pltpu.roll(prod, length - 1, axis=0),
    )
    conv = (
        taps[0:1] * prev * column(same_prev)
        + taps[1:2] * prod
        + taps[2:3] * nxt * column(same_next)
    )
    mixed = (outer[...].astype(F32) * conv).astype(BF16)
    mix[...] = mixed.reshape(tp_size, rows, chan)
    other = 1 - tp
    swap = pltpu.make_async_remote_copy(
        src_ref=mix.at[other],
        dst_ref=mix_in,
        send_sem=mix_send,
        recv_sem=mix_recv,
        device_id=(sp, other),
        device_id_type=MESH,
    )
    swap.start()
    loads[0].wait()
    tile = 512
    own = mix[tp]
    for c in range(0, width, tile):
        resid[:, c : c + tile] = stream[:, c : c + tile].astype(F32) + dot(
            own, ow[pl.ds(pl.multiple_of(tp * chan, chan), chan), c : c + tile]
        )
    swap.wait()
    theirs = mix_in[...]
    squares = jnp.zeros((rows, 1), F32)
    for c in range(0, width, tile):
        part = resid[:, c : c + tile] + dot(
            theirs, ow[pl.ds(pl.multiple_of(other * chan, chan), chan), c : c + tile]
        )
        resid[:, c : c + tile] = part
        squares = squares + jnp.sum(part * part, axis=1, keepdims=True)
    scale = lax.rsqrt(squares / width + 1e-06)
    for c in range(0, width, tile):
        normed[:, c : c + tile] = (
            resid[:, c : c + tile] * scale * gain[:, c : c + tile]
        ).astype(BF16)

    def start_group(src, dst, h, source_sem, target_sem):
        def one(i, carry):
            peer = (p + i) % per_plane
            pltpu.make_async_remote_copy(
                src_ref=src.at[peer],
                dst_ref=dst.at[p],
                send_sem=source_sem,
                recv_sem=target_sem,
                device_id=place(near(z, h) * per_plane + peer),
                device_id_type=MESH,
            ).start()
            return carry

        lax.fori_loop(1 - h, per_plane, one, 0)

    def wait_group(buf, h, sem):
        span = buf if h else buf.at[pl.ds(0, per_plane - 1)]
        pltpu.make_async_copy(span, span, sem).wait()

    def keep_in(q):
        return pltpu.make_async_copy(send.at[2 * q, p], recv.at[2 * q, p], self_sem.at[q])

    def keep_back(q, c):
        return pltpu.make_async_copy(
            outb.at[c, 2 * q, p], ret.at[c, 2 * q, p], self_back.at[PARTS * q + c]
        )

    tile = width // PARTS

    def dispatch(q, h, source, named_ids):
        g = 2 * q + h
        named, hits, spread = slots(near(z, h), named_ids)
        pick = spread(named).astype(BF16)
        for c in range(0, width, tile):
            send[g, :, :, c : c + tile] = (
                dot(pick, source[:, c : c + tile])
                .astype(BF16)
                .reshape(per_plane, cap, tile)
            )
        start_group(send.at[g], recv.at[g], h, out_sem.at[g], in_sem.at[g])
        if h == 0:
            keep_in(q).start()

    def experts(q, each):
        keep_in(q).wait()
        for h in range(2):
            wait_group(recv.at[2 * q + h], h, in_sem.at[2 * q + h])
        count = 2 * per_plane * cap
        x = recv[2 * q : 2 * q + 2].reshape(count, width)
        ff = hidden.shape[1]
        for f in range(0, ff, 256):
            a = dot(x, wg[:, f : f + 256])
            b = dot(x, wu[:, f : f + 256])
            hidden[:, f : f + 256] = (a / (1.0 + jnp.exp(-a)) * b).astype(BF16)
        for c in range(PARTS):
            outb[c, 2 * q : 2 * q + 2] = (
                dot(hidden[...], wd[:, c * tile : (c + 1) * tile])
                .astype(BF16)
                .reshape(2, per_plane, cap, tile)
            )
            each(q, c)

    def give_back(q, c):
        for h in (1, 0):
            g, at = 2 * q + h, 4 * c + 2 * q + h
            start_group(outb.at[c, g], ret.at[c, g], h, back_sem.at[at], home_sem.at[at])
        keep_back(q, c).start()

    def take_back(q, c):
        keep_back(q, c).wait()
        for h in range(2):
            wait_group(ret.at[c, 2 * q + h], h, home_sem.at[4 * c + 2 * q + h])

    def picks_of(named_ids):
        spreads = [slots(near(z, h), named_ids) for h in range(2)]
        return [
            jnp.concatenate(
                [jnp.transpose(spread(hits[k])) for _, hits, spread in spreads], axis=1
            ).astype(BF16)
            for k in range(top)
        ]

    def combined(q, c, picks, gates):
        given = ret[c, 2 * q : 2 * q + 2].reshape(2 * per_plane * cap, tile)
        return sum(gate * dot(pick, given) for gate, pick in zip(gates, picks))

    dispatch(0, 1, normed, ids)
    whole = to_mirror(normed, far, far_send.at[3], far_recv.at[3])
    whole.start()
    dispatch(0, 0, normed, ids)
    for load in loads[1:]:
        load.wait()
    for route in routes:
        route.wait()

    experts(0, lambda q, c: None)
    whole.wait()
    dispatch(1, 1, far, far_ids)
    dispatch(1, 0, far, far_ids)
    far_picks, far_gates = picks_of(far_ids), gate_columns(far_logits, far_weight)
    experts(1, give_back)
    for c in range(PARTS):
        give_back(0, c)

    parts = [
        to_mirror(halves.at[c], part_in.at[c], part_send.at[c], part_recv.at[c])
        for c in range(PARTS)
    ]
    for c in range(PARTS):
        take_back(1, c)
        halves[c] = combined(1, c, far_picks, far_gates).astype(BF16)
        parts[c].start()
    picks, gates = picks_of(ids), gate_columns(logits, weight)
    for c in range(PARTS):
        take_back(0, c)
        resid[:, c * tile : (c + 1) * tile] += combined(0, c, picks, gates)
    for c in range(PARTS):
        parts[c].wait()
        out[:, c * tile : (c + 1) * tile] = (
            resid[:, c * tile : (c + 1) * tile] + part_in[c].astype(F32)
        ).astype(BF16)

    for g in range(4):
        wait_group(send.at[g], g % 2, out_sem.at[g])
        for c in range(PARTS):
            wait_group(outb.at[c, g], g % 2, back_sem.at[4 * c + g])


def fused(
    tp_size, planes, per_plane, cap,
    stream, outer_gate, inner_gate, conv_values, doc_ids, conv_taps, out_weight, norm_gain,
    route_ids, route_logits, group_weight, w_gate, w_up, w_down,
):
    rows, width = stream.shape
    length, chan = inner_gate.shape
    ff = w_gate.shape[2]
    top = route_ids.shape[1]
    vmem = pl.BlockSpec(memory_space=pltpu.VMEM)
    anywhere = pl.BlockSpec(memory_space=pl.ANY)
    blocks = pltpu.VMEM((4, per_plane, cap, width), BF16)
    cut = pltpu.VMEM((PARTS, 4, per_plane, cap, width // PARTS), BF16)
    slab = pltpu.VMEM((PARTS, rows, width // PARTS), BF16)
    dma = pltpu.SemaphoreType.DMA
    return pl.pallas_call(
        functools.partial(fused_kernel, tp_size, planes, per_plane, cap),
        out_shape=jax.ShapeDtypeStruct((rows, width), BF16),
        in_specs=[vmem] * 10 + [anywhere] * 4,
        out_specs=vmem,
        scratch_shapes=[
            pltpu.VMEM(out_weight.shape, BF16),
            pltpu.VMEM((width, ff), BF16),
            pltpu.VMEM((width, ff), BF16),
            pltpu.VMEM((ff, width), BF16),
            pltpu.VMEM((2, 16, chan), BF16),
            pltpu.VMEM((2, 16, chan), BF16),
            pltpu.VMEM((2, 1, length), jnp.int32),
            pltpu.VMEM((tp_size, rows, chan), BF16),
            pltpu.VMEM((rows, chan), BF16),
            pltpu.VMEM((rows, width), F32),
            pltpu.VMEM((rows, width), BF16),
            pltpu.VMEM((2 * per_plane * cap, ff), BF16),
            blocks, blocks, cut, cut,
            pltpu.VMEM((rows, width), BF16),
            pltpu.VMEM((top, rows), jnp.int32),
            pltpu.VMEM((top, rows), F32),
            pltpu.VMEM((1, rows), F32),
            slab, slab,
            dma((4,)), dma((4,)), dma((4,)), dma, dma, dma((2,)), dma((2 * PARTS,)),
            dma((4,)), dma((4,)), dma((4 * PARTS,)), dma((4 * PARTS,)),
            dma((4,)), dma((4,)), dma((PARTS,)), dma((PARTS,)),
        ],
        compiler_params=pltpu.CompilerParams(
            collective_id=0, has_side_effects=True, vmem_limit_bytes=56 * 1024 * 1024
        ),
    )(
        stream, outer_gate, inner_gate, conv_values, doc_ids[None, :], conv_taps,
        norm_gain[None, :], route_ids.T, route_logits.T, group_weight[None, :],
        out_weight, w_gate, w_up, w_down,
    )


def body(*args):
    stream, route_ids = args[0], args[8]
    tp_size = lax.axis_size("tp")
    total = lax.axis_size("sp") * tp_size
    cap = 2 * stream.shape[0] * route_ids.shape[1] // total
    planes = 4
    per_plane = total // planes
    if tp_size != 2 or total % planes or cap % 16 or per_plane * cap != stream.shape[0]:
        return on_device(*args)
    return fused(tp_size, planes, per_plane, cap, *args)


def solution(mesh):
    placed = (
        P(("sp", "tp"), None),
        P("sp", "tp"),
        P("sp", "tp"),
        P("sp", "tp"),
        P("sp"),
        P(None, "tp"),
        P(),
        P(),
        P(("sp", "tp"), None),
        P(("sp", "tp"), None),
        P(("sp", "tp")),
        P(("sp", "tp"), None, None),
        P(("sp", "tp"), None, None),
        P(("sp", "tp"), None, None),
    )
    return jax.shard_map(
        body, mesh=mesh, in_specs=placed, out_specs=P(("sp", "tp"), None), check_vma=False
    )
```

profile of v0, /device:TPU:0, one launch (start us, length us, event | category | flops | bytes accessed | tf_op | source)
XLA Modules:
  0.0 98.2 jit_solution(1742452054245557336)
XLA Ops:
  0.0 96.3 %shard_map.136 = bf16[128,2048]{1,0:T(8,128)(2,1)} custom-call(bf16[128,2048]{1,0:T(8,128)(2,1)} %stream.1, bf16[256,512]{1,0:T(8,128)(2,1)} %outer.1, bf16[256,512]{1,0:T(8,128)(2,1)} %inner.1, bf16[256,512]{1,0:T(8,128)(2,1)} %values.1, s32[1,256]{1,0:T(1,128)} %bitcast.6, f32[3,512]{1,0:T(4,128)} %taps.1, f32[1,2048]{1,0:T(1,128)} %bitcast.5, ...), custom_call_target="tpu_custom_call" | custom-call | tf_op jit(solution)/shard_map/pallas_call | solution.py:451
  96.3 1.9 %copy.16 = bf16[128,2048]{1,0:T(8,128)(2,1)} copy(bf16[128,2048]{1,0:T(8,128)(2,1)} %shard_map.136) | data formatting | bytes 1048576
where the time goes:
time: 98.4 us; the launch traced here: 98.2 us
  Pallas kernels  96.3 us (98%)
  local copies, waits for them, and re-layouts  1.88 us (2%)
    pallas_call x1, Pallas kernels, fused(): pl.pallas_call(functools.partial(fused_kernel, tp_size, planes, per_plane...  96.3 us

commit v1 on v0

v1 whole, which is shorter than its diff:
```python
import functools

import jax
import jax.numpy as jnp
from jax import lax
from jax.experimental import pallas as pl
from jax.experimental.pallas import tpu as pltpu
from jax.sharding import PartitionSpec as P


def padded_2(shard, sides, width):
    for axis, dim in sides:
        size, length = (lax.axis_size(axis), shard.shape[dim])
        up = [(i, (i + 1) % size) for i in range(size - 1)]
        down = [(j, i) for i, j in up]
        last = lax.slice_in_dim(shard, length - width, length, axis=dim)
        leading = lax.slice_in_dim(shard, 0, width, axis=dim)
        before = lax.ppermute(last, axis, up)
        after = lax.ppermute(leading, axis, down)
        shard = jnp.concatenate([before, shard, after], axis=dim)
    return shard


def on_device(
    stream,
    outer_gate,
    inner_gate,
    conv_values,
    doc_ids,
    conv_taps,
    out_weight,
    norm_gain,
    route_ids,
    route_logits,
    group_weight,
    w_gate,
    w_up,
    w_down,
):
    tok_rows = stream.shape[0]
    width = stream.shape[1]
    product = (inner_gate.astype(jnp.float32) * conv_values.astype(jnp.float32)).astype(
        jnp.bfloat16
    )
    doc_float = doc_ids.astype(jnp.bfloat16)
    padded, padded_docs = (padded_2(product, (("sp", 0),), 1), padded_2(doc_float, (("sp", 0),), 1))
    same_prev = (padded_docs[:-2] == doc_float).astype(jnp.float32)[:, None]
    same_next = (padded_docs[2:] == doc_float).astype(jnp.float32)[:, None]
    conv = (
        conv_taps[0] * padded[:-2].astype(jnp.float32) * same_prev
        + conv_taps[1] * product.astype(jnp.float32)
        + conv_taps[2] * padded[2:].astype(jnp.float32) * same_next
    )
    mixed = (outer_gate.astype(jnp.float32) * conv).astype(jnp.bfloat16)
    channels = lax.all_to_all(mixed, "tp", split_axis=0, concat_axis=1, tiled=True)
    projected = jnp.dot(channels, out_weight, preferred_element_type=jnp.float32)
    resid = stream.astype(jnp.float32) + projected
    scale = lax.rsqrt(jnp.mean(resid * resid, axis=-1, keepdims=True) + 1e-06)
    normed = (resid * scale * norm_gain).astype(jnp.bfloat16)
    expert_total = lax.axis_size("sp") * lax.axis_size("tp")
    top_count = route_ids.shape[1]
    capacity = 2 * tok_rows * top_count // expert_total
    flat_ids = route_ids.reshape(-1)
    one_hot = (flat_ids[:, None] == jnp.arange(expert_total, dtype=jnp.int32)[None, :]).astype(
        jnp.int32
    )
    rank = jnp.sum((jnp.cumsum(one_hot, axis=0) - 1) * one_hot, axis=1)
    slot = flat_ids * capacity + rank
    slot_count = expert_total * capacity
    source_row = (
        jnp.zeros((slot_count,), jnp.int32)
        .at[slot]
        .set(jnp.arange(flat_ids.shape[0], dtype=jnp.int32) // top_count)
    )
    filled = jnp.zeros((slot_count,), jnp.bool_).at[slot].set(True)
    outgoing = jnp.where(filled[:, None], normed[source_row], jnp.zeros((), jnp.bfloat16)).reshape(
        expert_total, capacity, width
    )
    arrived = lax.all_to_all(outgoing, ("sp", "tp"), split_axis=0, concat_axis=0, tiled=True)
    sources, items, features = arrived.shape
    rows_in = arrived.reshape(sources * items, features)
    hidden = (
        jax.nn.silu(jnp.dot(rows_in, w_gate[0], preferred_element_type=jnp.float32))
        * jnp.dot(rows_in, w_up[0], preferred_element_type=jnp.float32)
    ).astype(jnp.bfloat16)
    outputs = jnp.dot(hidden, w_down[0], preferred_element_type=jnp.float32).astype(jnp.bfloat16)
    returned = lax.all_to_all(
        outputs.reshape(sources, items, features),
        ("sp", "tp"),
        split_axis=0,
        concat_axis=0,
        tiled=True,
    )
    picked = (
        returned.reshape(slot_count, width)[slot]
        .astype(jnp.float32)
        .reshape(tok_rows, top_count, width)
    )
    expo = jnp.exp(route_logits)
    gate = group_weight[:, None] * expo / jnp.sum(expo, axis=1, keepdims=True)
    result = resid + jnp.sum(gate[:, :, None] * picked, axis=1)
    return result.astype(jnp.bfloat16)


MESH = pl.DeviceIdType.MESH
F32, BF16 = jnp.float32, jnp.bfloat16


def dot(a, b):
    return jnp.dot(a, b, preferred_element_type=F32)


PARTS = 4


def fused_kernel(
    tp_size, planes, per_plane, cap,
    stream, outer, inner, values, docs, taps, gain, ids, logits, weight,
    ow_hbm, wg_hbm, wu_hbm, wd_hbm,
    out,
    ow, wg, wu, wd, edge_out, edge_in, doc_in, mix, mix_in, resid,
    meta, block, send, recv, outb, ret, acc_gate, acc_up, hidden, local, part_out, part_in,
    load_sem, edge_send, edge_recv, mix_send, mix_recv, meta_send, meta_recv,
    in_send, out_send, hop_recv, disp_send, disp_recv, back_send, back_recv,
    part_send, part_recv,
):
    sp, tp = lax.axis_index("sp"), lax.axis_index("tp")
    sp_size = planes * per_plane // tp_size
    total = planes * per_plane
    me = sp * tp_size + tp
    z, p = me // per_plane, me % per_plane
    rows, width = stream.shape
    chan = inner.shape[1]
    length = inner.shape[0]
    tile = width // PARTS
    top = ids.shape[0]
    ff = hidden.shape[1]

    middle = (z % 3 + 1) // 2
    is_middle, is_end = middle == 1, middle == 0
    step = 1 - 2 * (z // 2)
    order = [z, z + step * (1 - 2 * middle), z + step * (3 - middle), z + step * (2 - middle)]

    def place(index):
        return (index // tp_size, index % tp_size)

    inward = place((z + step) * per_plane + p)
    outward = place((z - step) * per_plane + p)

    def remote(src, dst, source_sem, target_sem, device):
        return pltpu.make_async_remote_copy(
            src_ref=src, dst_ref=dst, send_sem=source_sem, recv_sem=target_sem,
            device_id=device, device_id_type=MESH,
        )

    def wait_for(ref, sem):
        pltpu.make_async_copy(ref, ref, sem).wait()

    loads = [
        pltpu.make_async_copy(src, dst, load_sem.at[i])
        for i, (src, dst) in enumerate(
            ((ow_hbm, ow), (wg_hbm.at[0], wg), (wu_hbm.at[0], wu), (wd_hbm.at[0], wd))
        )
    ]
    for load in loads:
        load.start()

    barrier = pltpu.get_barrier_semaphore()

    def greet(i, carry):
        pl.semaphore_signal(
            barrier, inc=1, device_id=place((me + i) % total), device_id_type=MESH
        )
        return carry

    lax.fori_loop(1, total, greet, 0)
    product = (inner[...].astype(F32) * values[...].astype(F32)).astype(BF16)
    edge_out[0] = product[:16]
    edge_out[1] = product[length - 16 :]
    expo = jnp.exp(logits[...])
    gates = weight[...] * expo / jnp.sum(expo, axis=0, keepdims=True)
    meta[z] = jnp.concatenate([ids[...].astype(F32), gates, ids[...].astype(F32), gates], axis=0)
    pl.semaphore_wait(barrier, total - 1)

    left, right = ((sp + sp_size - 1) % sp_size, tp), ((sp + 1) % sp_size, tp)
    edges = []
    for side, (dest, src) in enumerate(((right, edge_out.at[1]), (left, edge_out.at[0]))):
        for kind, (source, target) in enumerate(
            ((src, edge_in.at[side]), (docs, doc_in.at[side]))
        ):
            at = 2 * side + kind
            edges.append(remote(source, target, edge_send.at[at], edge_recv.at[at], dest))
    for edge in edges:
        edge.start()

    metas = []
    for d in range(1, planes):
        there = place((z + d) % planes * per_plane + p)
        metas.append(remote(meta.at[z], meta.at[z], meta_send.at[d - 1], meta_recv.at[z], there))
    for copy in metas:
        copy.start()

    before = (
        lax.broadcasted_iota(jnp.int32, (rows, rows), 0)
        < lax.broadcasted_iota(jnp.int32, (rows, rows), 1)
    ).astype(F32).astype(BF16)
    rank_of = lax.broadcasted_iota(jnp.int32, (per_plane, cap, rows), 1).astype(F32)
    expert = (
        lax.broadcasted_iota(jnp.int32, (per_plane, rows), 0) + z * per_plane
    ).astype(F32)

    def slots(i):
        table = meta[order[i]]
        hits = [(table[k : k + 1] == expert).astype(F32) for k in range(top)]
        named = sum(hits)
        ahead = dot(named.astype(BF16), before)

        def spread(hit):
            at = jnp.where(hit > 0, ahead, -1.0)
            grid = jnp.broadcast_to(at[:, None, :], (per_plane, cap, rows))
            return jnp.where(grid == rank_of, 1.0, 0.0).reshape(per_plane * cap, rows)

        return named, hits, spread

    def to_slots(i):
        named, _, spread = slots(i)
        return spread(named).astype(BF16)

    def from_slots(i):
        _, hits, spread = slots(i)
        return [jnp.transpose(spread(hit)).astype(BF16) for hit in hits]

    def gate_columns(i):
        table = meta[order[i]]
        return [
            jnp.transpose(jnp.broadcast_to(table[top + k : top + k + 1], (rows, rows)))[:, :1]
            for k in range(top)
        ]

    picks = [to_slots(0)]

    for edge in edges:
        edge.wait()

    doc = jnp.broadcast_to(docs[...], (8, length))
    lane = lax.broadcasted_iota(jnp.int32, (8, length), 1)
    prior = jnp.where(
        lane == 0,
        pltpu.roll(jnp.broadcast_to(doc_in[0], (8, length)), 1, axis=1),
        pltpu.roll(doc, 1, axis=1),
    )
    later = jnp.where(
        lane == length - 1,
        pltpu.roll(jnp.broadcast_to(doc_in[1], (8, length)), length - 1, axis=1),
        pltpu.roll(doc, length - 1, axis=1),
    )
    spot = lane + sp * length
    same_prev = jnp.where((prior == doc) & (spot > 0), 1.0, 0.0)
    same_next = jnp.where((later == doc) & (spot < sp_size * length - 1), 1.0, 0.0)

    def column(row):
        return jnp.transpose(jnp.broadcast_to(row[:1], (128, length)))[:, :1]

    prod = product.astype(F32)
    row_at = lax.broadcasted_iota(jnp.int32, (length, chan), 0)
    prev = jnp.where(row_at == 0, edge_in[0].astype(F32)[15:16], pltpu.roll(prod, 1, axis=0))
    nxt = jnp.where(
        row_at == length - 1,
        edge_in[1].astype(F32)[:1],
        pltpu.roll(prod, length - 1, axis=0),
    )
    conv = (
        taps[0:1] * prev * column(same_prev)
        + taps[1:2] * prod
        + taps[2:3] * nxt * column(same_next)
    )
    mixed = (outer[...].astype(F32) * conv).astype(BF16)
    mix[...] = mixed.reshape(tp_size, rows, chan)
    other = 1 - tp
    swap = remote(mix.at[other], mix_in, mix_send, mix_recv, (sp, other))
    swap.start()
    loads[0].wait()
    own = mix[tp]
    for c in range(PARTS):
        cols = slice(c * tile, (c + 1) * tile)
        resid[c] = stream[:, cols].astype(F32) + dot(
            own, ow[pl.ds(pl.multiple_of(tp * chan, chan), chan), cols]
        )
    swap.wait()
    theirs = mix_in[...]
    squares = jnp.zeros((rows, 1), F32)
    for c in range(PARTS):
        cols = slice(c * tile, (c + 1) * tile)
        part = resid[c] + dot(
            theirs, ow[pl.ds(pl.multiple_of(other * chan, chan), chan), cols]
        )
        resid[c] = part
        squares = squares + jnp.sum(part * part, axis=1, keepdims=True)
    scale = lax.rsqrt(squares / width + 1e-06)

    def hop(j, c, sem, device):
        return remote(block.at[j, c], block.at[j, c], sem, hop_recv.at[j, c], device)

    def own_in(c):
        return hop(z, c, in_send.at[0, c], inward)

    def own_out(c):
        return hop(z, c, out_send.at[0, c], outward)

    def onward(i, c):
        if i == 1:
            return hop(order[1], c, in_send.at[1, c], inward)
        return hop(order[i], c, out_send.at[i - 1, c], outward)

    def forward(i, c):
        @pl.when(is_middle)
        def _():
            wait_for(block.at[order[i], c], hop_recv.at[order[i], c])
            onward(i, c).start()

    def group(src, dst, source_sem, target_sem):
        def one(i, carry):
            peer = (p + i) % per_plane
            remote(
                src.at[peer], dst.at[p], source_sem, target_sem, place(z * per_plane + peer)
            ).start()
            return carry

        lax.fori_loop(1, per_plane, one, 0)

    def wait_group(buf, sem):
        wait_for(buf.at[pl.ds(0, per_plane - 1)], sem)

    def dispatch(i, c):
        if i > 0:

            @pl.when(is_end)
            def _():
                wait_for(block.at[order[i], c], hop_recv.at[order[i], c])

        send[i, c] = (
            dot(picks[i], block[order[i], c]).astype(BF16).reshape(per_plane, cap, tile)
        )
        group(send.at[i, c], recv.at[i, c], disp_send.at[i, c], disp_recv.at[i, c])
        recv[i, c, p] = send[i, c, p]

    def upward(i, c):
        wait_group(recv.at[i, c], disp_recv.at[i, c])
        x = recv[i, c].reshape(per_plane * cap, tile)
        for f in range(0, ff, 256):
            a = dot(x, wg[c * tile : (c + 1) * tile, f : f + 256])
            b = dot(x, wu[c * tile : (c + 1) * tile, f : f + 256])
            if c > 0:
                a = acc_gate[:, f : f + 256] + a
                b = acc_up[:, f : f + 256] + b
            if c < PARTS - 1:
                acc_gate[:, f : f + 256] = a
                acc_up[:, f : f + 256] = b
            else:
                hidden[:, f : f + 256] = (a / (1.0 + jnp.exp(-a)) * b).astype(BF16)

    def downward(i):
        for c in range(PARTS):
            outb[i, c] = (
                dot(hidden[...], wd[:, c * tile : (c + 1) * tile])
                .astype(BF16)
                .reshape(per_plane, cap, tile)
            )
            group(outb.at[i, c], ret.at[i, c], back_send.at[i, c], back_recv.at[i, c])
            ret[i, c, p] = outb[i, c, p]

    spread_back = {}

    def part_copy(i, c, slot, device):
        return remote(
            part_out.at[i - 1, c], part_in.at[slot, c],
            part_send.at[i - 1, c], part_recv.at[slot, c], device,
        )

    def combine(i, c):
        if i not in spread_back:
            spread_back[i] = (from_slots(i), gate_columns(i))
        wait_group(ret.at[i, c], back_recv.at[i, c])
        given = ret[i, c].reshape(per_plane * cap, tile)
        part = sum(gate * dot(pick, given) for pick, gate in zip(*spread_back[i]))
        if i == 0:
            resid[c] += part
            return

        @pl.when(is_end)
        def _():
            part_out[i - 1, c] = part.astype(BF16)
            part_copy(i, c, planes if i == 1 else order[i], inward).start()

        @pl.when(is_middle)
        def _():
            local[i - 1, c] = part

    def relay(i, c):
        wait_for(part_in.at[order[i], c], part_recv.at[order[i], c])
        part_out[i - 1, c] = (local[i - 1, c] + part_in[order[i], c].astype(F32)).astype(BF16)
        part_copy(i, c, order[i], outward if i == 1 else inward).start()

    def finish(c, both):
        part = resid[c]
        if both:
            wait_for(part_in.at[planes, c], part_recv.at[planes, c])
            part = part + part_in[planes, c].astype(F32)
        wait_for(part_in.at[z, c], part_recv.at[z, c])
        out[:, c * tile : (c + 1) * tile] = (part + part_in[z, c].astype(F32)).astype(BF16)

    for c in range(PARTS):
        block[z, c] = (
            resid[c] * scale * gain[:, c * tile : (c + 1) * tile]
        ).astype(BF16)

        if c < 2:
            own_in(c).start()
        else:

            @pl.when(is_end)
            def _():
                own_in(c).start()

        @pl.when(is_middle)
        def _():
            own_out(c).start()

        dispatch(0, c)

    for i in range(1, planes):
        wait_for(meta.at[order[i]], meta_recv.at[order[i]])
    for load in loads[1:3]:
        load.wait()
    picks.append(to_slots(1))
    upward(0, 0)
    forward(1, 0)
    dispatch(1, 0)
    upward(0, 1)
    upward(0, 2)
    forward(1, 1)
    dispatch(1, 1)
    upward(0, 3)
    loads[3].wait()
    downward(0)
    forward(1, 2)
    dispatch(1, 2)
    forward(2, 0)
    picks.append(to_slots(2))
    combine(0, 0)
    upward(1, 0)
    forward(1, 3)

    @pl.when(is_middle)
    def _():
        for c in range(2, PARTS):
            own_in(c).start()

    dispatch(1, 3)
    forward(2, 1)
    combine(0, 1)
    combine(0, 2)
    upward(1, 1)
    forward(2, 2)
    combine(0, 3)
    upward(1, 2)
    dispatch(2, 0)
    upward(1, 3)
    downward(1)
    forward(2, 3)
    forward(3, 0)
    forward(3, 1)
    dispatch(2, 1)
    picks.append(to_slots(3))
    combine(1, 0)
    upward(2, 0)
    combine(1, 1)
    dispatch(2, 2)
    forward(3, 2)
    combine(1, 2)
    upward(2, 1)
    combine(1, 3)
    dispatch(2, 3)
    forward(3, 3)
    upward(2, 2)
    dispatch(3, 0)
    upward(2, 3)
    downward(2)
    dispatch(3, 1)
    combine(2, 0)
    upward(3, 0)
    combine(2, 1)
    dispatch(3, 2)
    combine(2, 2)
    upward(3, 1)
    combine(2, 3)
    dispatch(3, 3)
    upward(3, 2)
    upward(3, 3)
    downward(3)
    for c in range(PARTS):
        combine(3, c)

    @pl.when(is_end)
    def _():
        for c in range(PARTS):
            finish(c, False)

    @pl.when(is_middle)
    def _():
        for i, c in (
            (2, 0), (2, 1), (1, 0), (2, 2), (1, 1), (2, 3), (1, 2), (3, 0), (1, 3), (3, 1),
            (0, 0), (3, 2), (0, 1), (3, 3), (0, 2), (0, 3),
        ):
            if i:
                relay(i, c)
            else:
                finish(c, True)

    for copy in metas:
        copy.wait_send()
    for c in range(PARTS):
        own_in(c).wait_send()
        for i in range(planes):
            wait_group(send.at[i, c], disp_send.at[i, c])
            wait_group(outb.at[i, c], back_send.at[i, c])
        for i in range(1, planes):
            wait_for(part_out.at[i - 1, c], part_send.at[i - 1, c])

    @pl.when(is_middle)
    def _():
        for c in range(PARTS):
            own_out(c).wait_send()
            for i in range(1, planes):
                onward(i, c).wait_send()


def fused(
    tp_size, planes, per_plane, cap,
    stream, outer_gate, inner_gate, conv_values, doc_ids, conv_taps, out_weight, norm_gain,
    route_ids, route_logits, group_weight, w_gate, w_up, w_down,
):
    rows, width = stream.shape
    length, chan = inner_gate.shape
    ff = w_gate.shape[2]
    tile = width // PARTS
    vmem = pl.BlockSpec(memory_space=pltpu.VMEM)
    anywhere = pl.BlockSpec(memory_space=pl.ANY)
    slotted = pltpu.VMEM((planes, PARTS, per_plane, cap, tile), BF16)
    dma = pltpu.SemaphoreType.DMA
    return pl.pallas_call(
        functools.partial(fused_kernel, tp_size, planes, per_plane, cap),
        out_shape=jax.ShapeDtypeStruct((rows, width), BF16),
        in_specs=[vmem] * 10 + [anywhere] * 4,
        out_specs=vmem,
        scratch_shapes=[
            pltpu.VMEM(out_weight.shape, BF16),
            pltpu.VMEM((width, ff), BF16),
            pltpu.VMEM((width, ff), BF16),
            pltpu.VMEM((ff, width), BF16),
            pltpu.VMEM((2, 16, chan), BF16),
            pltpu.VMEM((2, 16, chan), BF16),
            pltpu.VMEM((2, 1, length), jnp.int32),
            pltpu.VMEM((tp_size, rows, chan), BF16),
            pltpu.VMEM((rows, chan), BF16),
            pltpu.VMEM((PARTS, rows, tile), F32),
            pltpu.VMEM((planes, 8, rows), F32),
            pltpu.VMEM((planes, PARTS, rows, tile), BF16),
            slotted, slotted, slotted, slotted,
            pltpu.VMEM((per_plane * cap, ff), F32),
            pltpu.VMEM((per_plane * cap, ff), F32),
            pltpu.VMEM((per_plane * cap, ff), BF16),
            pltpu.VMEM((planes - 1, PARTS, rows, tile), F32),
            pltpu.VMEM((planes - 1, PARTS, rows, tile), BF16),
            pltpu.VMEM((planes + 1, PARTS, rows, tile), BF16),
            dma((4,)), dma((4,)), dma((4,)), dma, dma, dma((planes - 1,)), dma((planes,)),
            dma((2, PARTS)), dma((3, PARTS)), dma((planes, PARTS)),
            dma((planes, PARTS)), dma((planes, PARTS)),
            dma((planes, PARTS)), dma((planes, PARTS)),
            dma((planes - 1, PARTS)), dma((planes + 1, PARTS)),
        ],
        compiler_params=pltpu.CompilerParams(
            collective_id=0, has_side_effects=True, vmem_limit_bytes=56 * 1024 * 1024
        ),
    )(
        stream, outer_gate, inner_gate, conv_values, doc_ids[None, :], conv_taps,
        norm_gain[None, :], route_ids.T, route_logits.T, group_weight[None, :],
        out_weight, w_gate, w_up, w_down,
    )


def body(*args):
    stream, route_ids = args[0], args[8]
    tp_size = lax.axis_size("tp")
    total = lax.axis_size("sp") * tp_size
    top = route_ids.shape[1]
    cap = 2 * stream.shape[0] * top // total
    planes = 4
    per_plane = total // planes
    if tp_size != 2 or top != 2 or total % planes or cap % 16 or per_plane * cap != stream.shape[0]:
        return on_device(*args)
    return fused(tp_size, planes, per_plane, cap, *args)


def solution(mesh):
    placed = (
        P(("sp", "tp"), None),
        P("sp", "tp"),
        P("sp", "tp"),
        P("sp", "tp"),
        P("sp"),
        P(None, "tp"),
        P(),
        P(),
        P(("sp", "tp"), None),
        P(("sp", "tp"), None),
        P(("sp", "tp")),
        P(("sp", "tp"), None, None),
        P(("sp", "tp"), None, None),
        P(("sp", "tp"), None, None),
    )
    return jax.shard_map(
        body, mesh=mesh, in_specs=placed, out_specs=P(("sp", "tp"), None), check_vma=False
    )
```

time: 98.4 us -> 99.9 us (1.015)
  the two profiles are of different devices: /device:TPU:0 before, /device:TPU:8 now
where the time goes in v1:
time: 99.9 us; the launch traced here: 99.7 us
  Pallas kernels  97.8 us (98%)
  local copies, waits for them, and re-layouts  1.88 us (2%)
    pallas_call x1, Pallas kernels, fused(): pl.pallas_call(functools.partial(fused_kernel, tp_size, planes, per_plane...  97.8 us

profile of v1, /device:TPU:8, one launch (start us, length us, event | category | flops | bytes accessed | tf_op | source)
XLA Modules:
  0.0 99.7 jit_solution(17860521223897369270)
XLA Ops:
  0.0 97.8 %shard_map.136 = bf16[128,2048]{1,0:T(8,128)(2,1)} custom-call(bf16[128,2048]{1,0:T(8,128)(2,1)} %stream.1, bf16[256,512]{1,0:T(8,128)(2,1)} %outer.1, bf16[256,512]{1,0:T(8,128)(2,1)} %inner.1, bf16[256,512]{1,0:T(8,128)(2,1)} %values.1, s32[1,256]{1,0:T(1,128)} %bitcast.6, f32[3,512]{1,0:T(4,128)} %taps.1, f32[1,2048]{1,0:T(1,128)} %bitcast.5, ...), custom_call_target="tpu_custom_call" | custom-call | tf_op jit(solution)/shard_map/pallas_call | solution.py:551
  97.8 1.9 %copy.16 = bf16[128,2048]{1,0:T(8,128)(2,1)} copy(bf16[128,2048]{1,0:T(8,128)(2,1)} %shard_map.136) | data formatting | bytes 1048576

commit v2 on v1

--- a/solution.py
+++ b/solution.py
@@ -115,14 +115,15 @@
 
 def fused_kernel(
     tp_size, planes, per_plane, cap,
-    stream, outer, inner, values, docs, taps, gain, ids, logits, weight,
-    ow_hbm, wg_hbm, wu_hbm, wd_hbm,
+    docs, taps, gain, ids, logits, weight,
+    inner_hbm, values_hbm, outer_hbm, stream_hbm, ow_hbm, wg_hbm, wu_hbm, wd_hbm,
     out,
-    ow, wg, wu, wd, edge_out, edge_in, doc_in, mix, mix_in, resid,
+    inner, values, outer, stream, ow, wg, wu, wd,
+    product, product_in, outer_in, taps_in, edge_out, edge_in, doc_in, resid, result,
     meta, block, send, recv, outb, ret, acc_gate, acc_up, hidden, local, part_out, part_in,
-    load_sem, edge_send, edge_recv, mix_send, mix_recv, meta_send, meta_recv,
+    load_sem, edge_send, edge_recv, swap_send, swap_recv, meta_send, meta_recv,
     in_send, out_send, hop_recv, disp_send, disp_recv, back_send, back_recv,
-    part_send, part_recv,
+    part_send, part_recv, result_sem,
 ):
     sp, tp = lax.axis_index("sp"), lax.axis_index("tp")
     sp_size = planes * per_plane // tp_size
@@ -130,11 +131,11 @@
     me = sp * tp_size + tp
     z, p = me // per_plane, me % per_plane
     rows, width = stream.shape
-    chan = inner.shape[1]
-    length = inner.shape[0]
+    length, chan = inner.shape
     tile = width // PARTS
     top = ids.shape[0]
     ff = hidden.shape[1]
+    other = 1 - tp
 
     middle = (z % 3 + 1) // 2
     is_middle, is_end = middle == 1, middle == 0
@@ -159,39 +160,90 @@
     loads = [
         pltpu.make_async_copy(src, dst, load_sem.at[i])
         for i, (src, dst) in enumerate(
-            ((ow_hbm, ow), (wg_hbm.at[0], wg), (wu_hbm.at[0], wu), (wd_hbm.at[0], wd))
+            (
+                (inner_hbm, inner), (values_hbm, values), (outer_hbm, outer),
+                (stream_hbm, stream), (ow_hbm, ow),
+                (wg_hbm.at[0], wg), (wu_hbm.at[0], wu), (wd_hbm.at[0], wd),
+            )
         )
     ]
     for load in loads:
         load.start()
 
+    has_left, has_right = sp > 0, sp < sp_size - 1
     barrier = pltpu.get_barrier_semaphore()
 
-    def greet(i, carry):
-        pl.semaphore_signal(
-            barrier, inc=1, device_id=place((me + i) % total), device_id_type=MESH
-        )
-        return carry
-
-    lax.fori_loop(1, total, greet, 0)
-    product = (inner[...].astype(F32) * values[...].astype(F32)).astype(BF16)
-    edge_out[0] = product[:16]
-    edge_out[1] = product[length - 16 :]
+    def greet(device):
+        pl.semaphore_signal(barrier, inc=1, device_id=device, device_id_type=MESH)
+
+    @pl.when((tp == 0) & has_left)
+    def _():
+        for q in range(tp_size):
+            greet((sp - 1, q))
+
+    @pl.when((tp == 1) & has_right)
+    def _():
+        for q in range(tp_size):
+            greet((sp + 1, q))
+
+    for d in range(1, planes):
+        greet(place((z + d) % planes * per_plane + p))
+    for d in range(1, per_plane):
+        greet(place(z * per_plane + (p + d) % per_plane))
+
     expo = jnp.exp(logits[...])
     gates = weight[...] * expo / jnp.sum(expo, axis=0, keepdims=True)
     meta[z] = jnp.concatenate([ids[...].astype(F32), gates, ids[...].astype(F32), gates], axis=0)
-    pl.semaphore_wait(barrier, total - 1)
-
-    left, right = ((sp + sp_size - 1) % sp_size, tp), ((sp + 1) % sp_size, tp)
-    edges = []
-    for side, (dest, src) in enumerate(((right, edge_out.at[1]), (left, edge_out.at[0]))):
-        for kind, (source, target) in enumerate(
-            ((src, edge_in.at[side]), (docs, doc_in.at[side]))
-        ):
-            at = 2 * side + kind
-            edges.append(remote(source, target, edge_send.at[at], edge_recv.at[at], dest))
-    for edge in edges:
-        edge.start()
+
+    @pl.when(((tp == 0) & (sp == 0)) | ((tp == 1) & (sp == sp_size - 1)))
+    def _():
+        edge_in[...] = jnp.zeros_like(edge_in)
+        doc_in[...] = jnp.zeros_like(doc_in)
+
+    for load in loads[:2]:
+        load.wait()
+    product[...] = (inner[...].astype(F32) * values[...].astype(F32)).astype(BF16)
+    edge_out[0] = product[:16]
+    edge_out[1] = product[length - 16 :]
+    loads[2].wait()
+    pl.semaphore_wait(
+        barrier,
+        planes + per_plane - 2 + (sp + sp_size - 1) // sp_size + (2 * sp_size - 2 - sp) // sp_size,
+    )
+
+    def edge_copies(side, device):
+        return [
+            remote(
+                source, target.at[tp], edge_send.at[2 * side + kind], edge_recv.at[tp, kind], device
+            )
+            for kind, (source, target) in enumerate(((edge_out.at[side], edge_in), (docs, doc_in)))
+        ]
+
+    to_right, to_left = edge_copies(1, (sp + 1, 0)), edge_copies(0, (sp - 1, 1))
+
+    @pl.when(has_right)
+    def _():
+        for copy in to_right:
+            copy.start()
+
+    @pl.when(has_left)
+    def _():
+        for copy in to_left:
+            copy.start()
+
+    span = rows + 16
+    swaps = [
+        remote(src, dst, swap_send.at[i], swap_recv.at[i], (sp, other))
+        for i, (src, dst) in enumerate(
+            (
+                (product.at[pl.ds(pl.multiple_of(other * (rows - 16), 16), span)], product_in),
+                (outer.at[pl.ds(pl.multiple_of(other * rows, rows), rows)], outer_in),
+                (taps, taps_in),
+            )
+        )
+    ]
+    for copy in swaps:
+        copy.start()
 
     metas = []
     for d in range(1, planes):
@@ -239,60 +291,61 @@
 
     picks = [to_slots(0)]
 
-    for edge in edges:
-        edge.wait()
+    row_at = lax.broadcasted_iota(jnp.int32, (rows, chan), 0)
+    prod = product[pl.ds(pl.multiple_of(tp * rows, rows), rows)].astype(F32)
+    seam = [product[rows - 16 : rows].astype(F32)[15:], product[rows : rows + 16].astype(F32)[:1]]
+    for copy in swaps:
+        copy.wait_recv()
+    prod_in = product_in[pl.ds(pl.multiple_of(tp * 16, 16), rows)].astype(F32)
+    seam_in = [product_in[:16].astype(F32)[15:], product_in[rows:].astype(F32)[:1]]
+
+    @pl.when(((tp == 0) & has_left) | ((tp == 1) & has_right))
+    def _():
+        for q in range(tp_size):
+            wait_for(edge_in.at[q], edge_recv.at[q, 0])
+            wait_for(doc_in.at[q], edge_recv.at[q, 1])
 
     doc = jnp.broadcast_to(docs[...], (8, length))
+    beyond = jnp.broadcast_to(doc_in[0], (8, length))
     lane = lax.broadcasted_iota(jnp.int32, (8, length), 1)
-    prior = jnp.where(
-        lane == 0,
-        pltpu.roll(jnp.broadcast_to(doc_in[0], (8, length)), 1, axis=1),
-        pltpu.roll(doc, 1, axis=1),
-    )
-    later = jnp.where(
-        lane == length - 1,
-        pltpu.roll(jnp.broadcast_to(doc_in[1], (8, length)), length - 1, axis=1),
-        pltpu.roll(doc, length - 1, axis=1),
-    )
+    prior = pltpu.roll(jnp.where(lane == length - 1, beyond, doc), 1, axis=1)
+    later = pltpu.roll(jnp.where(lane == 0, beyond, doc), length - 1, axis=1)
     spot = lane + sp * length
     same_prev = jnp.where((prior == doc) & (spot > 0), 1.0, 0.0)
     same_next = jnp.where((later == doc) & (spot < sp_size * length - 1), 1.0, 0.0)
 
     def column(row):
-        return jnp.transpose(jnp.broadcast_to(row[:1], (128, length)))[:, :1]
-
-    prod = product.astype(F32)
-    row_at = lax.broadcasted_iota(jnp.int32, (length, chan), 0)
-    prev = jnp.where(row_at == 0, edge_in[0].astype(F32)[15:16], pltpu.roll(prod, 1, axis=0))
-    nxt = jnp.where(
-        row_at == length - 1,
-        edge_in[1].astype(F32)[:1],
-        pltpu.roll(prod, length - 1, axis=0),
-    )
-    conv = (
-        taps[0:1] * prev * column(same_prev)
-        + taps[1:2] * prod
-        + taps[2:3] * nxt * column(same_next)
-    )
-    mixed = (outer[...].astype(F32) * conv).astype(BF16)
-    mix[...] = mixed.reshape(tp_size, rows, chan)
-    other = 1 - tp
-    swap = remote(mix.at[other], mix_in, mix_send, mix_recv, (sp, other))
-    swap.start()
-    loads[0].wait()
-    own = mix[tp]
-    for c in range(PARTS):
-        cols = slice(c * tile, (c + 1) * tile)
-        resid[c] = stream[:, cols].astype(F32) + dot(
-            own, ow[pl.ds(pl.multiple_of(tp * chan, chan), chan), cols]
-        )
-    swap.wait()
-    theirs = mix_in[...]
+        mine = jnp.where(tp == 0, row[:1, :rows], row[:1, rows:])
+        return jnp.transpose(jnp.broadcast_to(mine, (128, rows)))[:, :1]
+
+    before_col, after_col = column(same_prev), column(same_next)
+
+    def mix(values_f, ends, edge, weights, gate):
+        first = jnp.where(tp == 0, edge[15:], ends[0])
+        last = jnp.where(tp == 0, ends[1], edge[:1])
+        prev = jnp.where(row_at == 0, first, pltpu.roll(values_f, 1, axis=0))
+        nxt = jnp.where(row_at == rows - 1, last, pltpu.roll(values_f, rows - 1, axis=0))
+        conv = (
+            weights[0:1] * prev * before_col
+            + weights[1:2] * values_f
+            + weights[2:3] * nxt * after_col
+        )
+        return (gate.astype(F32) * conv).astype(BF16)
+
+    mine = mix(
+        prod, seam, edge_in[tp].astype(F32), taps[...],
+        outer[pl.ds(pl.multiple_of(tp * rows, rows), rows)],
+    )
+    theirs = mix(prod_in, seam_in, edge_in[other].astype(F32), taps_in[...], outer_in[...])
+    loads[3].wait()
+    loads[4].wait()
     squares = jnp.zeros((rows, 1), F32)
     for c in range(PARTS):
         cols = slice(c * tile, (c + 1) * tile)
-        part = resid[c] + dot(
-            theirs, ow[pl.ds(pl.multiple_of(other * chan, chan), chan), cols]
+        part = (
+            stream[:, cols].astype(F32)
+            + dot(mine, ow[pl.ds(pl.multiple_of(tp * chan, chan), chan), cols])
+            + dot(theirs, ow[pl.ds(pl.multiple_of(other * chan, chan), chan), cols])
         )
         resid[c] = part
         squares = squares + jnp.sum(part * part, axis=1, keepdims=True)
@@ -313,10 +366,8 @@
         return hop(order[i], c, out_send.at[i - 1, c], outward)
 
     def forward(i, c):
-        @pl.when(is_middle)
-        def _():
-            wait_for(block.at[order[i], c], hop_recv.at[order[i], c])
-            onward(i, c).start()
+        wait_for(block.at[order[i], c], hop_recv.at[order[i], c])
+        onward(i, c).start()
 
     def group(src, dst, source_sem, target_sem):
         def one(i, carry):
@@ -332,12 +383,8 @@
         wait_for(buf.at[pl.ds(0, per_plane - 1)], sem)
 
     def dispatch(i, c):
-        if i > 0:
-
-            @pl.when(is_end)
-            def _():
-                wait_for(block.at[order[i], c], hop_recv.at[order[i], c])
-
+        if i > 0 and not relaying[0]:
+            wait_for(block.at[order[i], c], hop_recv.at[order[i], c])
         send[i, c] = (
             dot(picks[i], block[order[i], c]).astype(BF16).reshape(per_plane, cap, tile)
         )
@@ -369,7 +416,7 @@
             group(outb.at[i, c], ret.at[i, c], back_send.at[i, c], back_recv.at[i, c])
             ret[i, c, p] = outb[i, c, p]
 
-    spread_back = {}
+    spread_back, relaying = {}, [False]
 
     def part_copy(i, c, slot, device):
         return remote(
@@ -387,19 +434,21 @@
             resid[c] += part
             return
 
-        @pl.when(is_end)
-        def _():
+        if relaying[0]:
+            local[i - 1, c] = part
+        else:
             part_out[i - 1, c] = part.astype(BF16)
             part_copy(i, c, planes if i == 1 else order[i], inward).start()
-
-        @pl.when(is_middle)
-        def _():
-            local[i - 1, c] = part
 
     def relay(i, c):
         wait_for(part_in.at[order[i], c], part_recv.at[order[i], c])
         part_out[i - 1, c] = (local[i - 1, c] + part_in[order[i], c].astype(F32)).astype(BF16)
         part_copy(i, c, order[i], outward if i == 1 else inward).start()
+
+    def deliver(c):
+        return pltpu.make_async_copy(
+            result.at[c], out.at[:, pl.ds(c * tile, tile)], result_sem.at[c]
+        )
 
     def finish(c, both):
         part = resid[c]
@@ -407,7 +456,8 @@
             wait_for(part_in.at[planes, c], part_recv.at[planes, c])
             part = part + part_in[planes, c].astype(F32)
         wait_for(part_in.at[z, c], part_recv.at[z, c])
-        out[:, c * tile : (c + 1) * tile] = (part + part_in[z, c].astype(F32)).astype(BF16)
+        result[c] = (part + part_in[z, c].astype(F32)).astype(BF16)
+        deliver(c).start()
 
     for c in range(PARTS):
         block[z, c] = (
@@ -430,95 +480,66 @@
 
     for i in range(1, planes):
         wait_for(meta.at[order[i]], meta_recv.at[order[i]])
-    for load in loads[1:3]:
+    for load in loads[5:7]:
         load.wait()
-    picks.append(to_slots(1))
-    upward(0, 0)
-    forward(1, 0)
-    dispatch(1, 0)
-    upward(0, 1)
-    upward(0, 2)
-    forward(1, 1)
-    dispatch(1, 1)
-    upward(0, 3)
-    loads[3].wait()
-    downward(0)
-    forward(1, 2)
-    dispatch(1, 2)
-    forward(2, 0)
-    picks.append(to_slots(2))
-    combine(0, 0)
-    upward(1, 0)
-    forward(1, 3)
-
-    @pl.when(is_middle)
-    def _():
+
+    def own_rest():
         for c in range(2, PARTS):
             own_in(c).start()
 
-    dispatch(1, 3)
-    forward(2, 1)
-    combine(0, 1)
-    combine(0, 2)
-    upward(1, 1)
-    forward(2, 2)
-    combine(0, 3)
-    upward(1, 2)
-    dispatch(2, 0)
-    upward(1, 3)
-    downward(1)
-    forward(2, 3)
-    forward(3, 0)
-    forward(3, 1)
-    dispatch(2, 1)
-    picks.append(to_slots(3))
-    combine(1, 0)
-    upward(2, 0)
-    combine(1, 1)
-    dispatch(2, 2)
-    forward(3, 2)
-    combine(1, 2)
-    upward(2, 1)
-    combine(1, 3)
-    dispatch(2, 3)
-    forward(3, 3)
-    upward(2, 2)
-    dispatch(3, 0)
-    upward(2, 3)
-    downward(2)
-    dispatch(3, 1)
-    combine(2, 0)
-    upward(3, 0)
-    combine(2, 1)
-    dispatch(3, 2)
-    combine(2, 2)
-    upward(3, 1)
-    combine(2, 3)
-    dispatch(3, 3)
-    upward(3, 2)
-    upward(3, 3)
-    downward(3)
-    for c in range(PARTS):
-        combine(3, c)
+    def run(plan, relays):
+        relaying[0] = relays
+        picks[1:] = []
+        spread_back.clear()
+        steps = {
+            "U": upward, "D": dispatch, "F": forward, "C": combine, "R": relay,
+            "E": lambda i, c: finish(c, i == 1),
+            "N": lambda i, c: downward(i),
+            "P": lambda i, c: picks.append(to_slots(i)),
+            "W": lambda i, c: loads[7].wait(),
+            "O": lambda i, c: own_rest(),
+        }
+        for name in " ".join(plan).split():
+            steps[name[0]](int(name[1]), int(name[2]))
 
     @pl.when(is_end)
     def _():
-        for c in range(PARTS):
-            finish(c, False)
+        run(
+            (
+                "U00 U01 U02 P10", "D10 U03 W00 N00", "D11 D12 C00 U10", "D13 U11 C01 C02",
+                "C03 U12 P20 D20", "U13 D21 N10 U20", "D22 U21 C10 D23", "C11 C12 P30 D30",
+                "C13 U22 D31 U23", "N20 D32 U30 U31", "C20 D33 C21 C22", "C23 U32 U33 N30",
+                "C30 C31 C32 C33", "E00 E01 E02 E03",
+            ),
+            False,
+        )
 
     @pl.when(is_middle)
     def _():
-        for i, c in (
-            (2, 0), (2, 1), (1, 0), (2, 2), (1, 1), (2, 3), (1, 2), (3, 0), (1, 3), (3, 1),
-            (0, 0), (3, 2), (0, 1), (3, 3), (0, 2), (0, 3),
-        ):
-            if i:
-                relay(i, c)
-            else:
-                finish(c, True)
-
-    for copy in metas:
+        run(
+            (
+                "P10 U00 F10 D10", "U01 U02 F11 D11", "U03 W00 N00 F12", "D12 P20 F20 D20",
+                "F13 O00 D13 F21", "D21 U10 U11 C00", "C01 F22 D22 C02", "C03 F23 D23 U12",
+                "P30 U13 N10 F30", "F31 D30 D31 U20", "U21 F32 D32 U22", "U23 F33 D33 N20",
+                "C10 C11 C12 C13", "U30 U31 U32 U33", "N30 C20 C21 R20", "C22 C23 R21 C30",
+                "R10 C31 R22 C32", "R11 C33 R23 R12", "R30 R13 R31 R32", "E10 R33 E11 E12", "E13",
+            ),
+            True,
+        )
+
+    for copy in metas + swaps:
         copy.wait_send()
+
+    @pl.when(has_right)
+    def _():
+        for copy in to_right:
+            copy.wait_send()
+
+    @pl.when(has_left)
+    def _():
+        for copy in to_left:
+            copy.wait_send()
+
     for c in range(PARTS):
         own_in(c).wait_send()
         for i in range(planes):
@@ -533,6 +554,9 @@
             own_out(c).wait_send()
             for i in range(1, planes):
                 onward(i, c).wait_send()
+
+    for c in range(PARTS):
+        deliver(c).wait()
 
 
 def fused(
@@ -551,19 +575,26 @@
     return pl.pallas_call(
         functools.partial(fused_kernel, tp_size, planes, per_plane, cap),
         out_shape=jax.ShapeDtypeStruct((rows, width), BF16),
-        in_specs=[vmem] * 10 + [anywhere] * 4,
-        out_specs=vmem,
+        in_specs=[vmem] * 6 + [anywhere] * 8,
+        out_specs=anywhere,
         scratch_shapes=[
+            pltpu.VMEM((length, chan), BF16),
+            pltpu.VMEM((length, chan), BF16),
+            pltpu.VMEM((length, chan), BF16),
+            pltpu.VMEM((rows, width), BF16),
             pltpu.VMEM(out_weight.shape, BF16),
             pltpu.VMEM((width, ff), BF16),
             pltpu.VMEM((width, ff), BF16),
             pltpu.VMEM((ff, width), BF16),
+            pltpu.VMEM((length, chan), BF16),
+            pltpu.VMEM((rows + 16, chan), BF16),
+            pltpu.VMEM((rows, chan), BF16),
+            pltpu.VMEM(conv_taps.shape, F32),
             pltpu.VMEM((2, 16, chan), BF16),
             pltpu.VMEM((2, 16, chan), BF16),
             pltpu.VMEM((2, 1, length), jnp.int32),
-            pltpu.VMEM((tp_size, rows, chan), BF16),
-            pltpu.VMEM((rows, chan), BF16),
             pltpu.VMEM((PARTS, rows, tile), F32),
+            pltpu.VMEM((PARTS, rows, tile), BF16),
             pltpu.VMEM((planes, 8, rows), F32),
             pltpu.VMEM((planes, PARTS, rows, tile), BF16),
             slotted, slotted, slotted, slotted,
@@ -573,19 +604,19 @@
             pltpu.VMEM((planes - 1, PARTS, rows, tile), F32),
             pltpu.VMEM((planes - 1, PARTS, rows, tile), BF16),
             pltpu.VMEM((planes + 1, PARTS, rows, tile), BF16),
-            dma((4,)), dma((4,)), dma((4,)), dma, dma, dma((planes - 1,)), dma((planes,)),
+            dma((8,)), dma((4,)), dma((2, 2)), dma((3,)), dma((3,)), dma((planes - 1,)), dma((planes,)),
             dma((2, PARTS)), dma((3, PARTS)), dma((planes, PARTS)),
             dma((planes, PARTS)), dma((planes, PARTS)),
             dma((planes, PARTS)), dma((planes, PARTS)),
-            dma((planes - 1, PARTS)), dma((planes + 1, PARTS)),
+            dma((planes - 1, PARTS)), dma((planes + 1, PARTS)), dma((PARTS,)),
         ],
         compiler_params=pltpu.CompilerParams(
             collective_id=0, has_side_effects=True, vmem_limit_bytes=56 * 1024 * 1024
         ),
     )(
-        stream, outer_gate, inner_gate, conv_values, doc_ids[None, :], conv_taps,
-        norm_gain[None, :], route_ids.T, route_logits.T, group_weight[None, :],
-        out_weight, w_gate, w_up, w_down,
+        doc_ids[None, :], conv_taps, norm_gain[None, :],
+        route_ids.T, route_logits.T, group_weight[None, :],
+        inner_gate, conv_values, outer_gate, stream, out_weight, w_gate, w_up, w_down,
     )
 
 

time: 99.9 us -> 81 us (0.81)
  Pallas kernels: 97.8 us -> 78.9 us
    pallas_call x1, Pallas kernels: 97.8 us -> 78.9 us  [fused(): pl.pallas_call(functools.partial(fused_kernel, tp_size, planes, per_plane...]
where the time goes in v2:
time: 81 us; the launch traced here: 80.8 us
  Pallas kernels  78.9 us (97%)
  local copies, waits for them, and re-layouts  1.88 us (2%)
    pallas_call x1, Pallas kernels, fused(): pl.pallas_call(functools.partial(fused_kernel, tp_size, planes, per_plane...  78.9 us
    unnamed x1, local copies, waits for them, and re-layouts  1.88 us

profile of v2, /device:TPU:8, one launch (start us, length us, event | category | flops | bytes accessed | tf_op | source)
XLA Modules:
  0.0 80.8 jit_solution(2588403884444141938)
XLA Ops:
  0.0 78.9 %shard_map.136 = bf16[128,2048]{1,0:T(8,128)(2,1)} custom-call(s32[1,256]{1,0:T(1,128)} %bitcast.6, f32[3,512]{1,0:T(4,128)} %taps.1, f32[1,2048]{1,0:T(1,128)} %bitcast.5, s32[2,128]{1,0:T(2,128)} %bitcast.7, f32[2,128]{1,0:T(2,128)} %bitcast.8, f32[1,128]{1,0:T(1,128)} %bitcast.9, bf16[256,512]{1,0:T(8,128)(2,1)} %inner_hbm.1, ...), custom_call_target="tpu_custom_call" | custom-call | tf_op jit(solution)/shard_map/pallas_call | solution.py:575
  78.9 1.9 %copy.16 = bf16[128,2048]{1,0:T(8,128)(2,1)} copy(bf16[128,2048]{1,0:T(8,128)(2,1)} %shard_map.136) | data formatting | bytes 1048576

commit v3 on v2

--- a/solution.py
+++ b/solution.py
@@ -299,20 +299,12 @@
     prod_in = product_in[pl.ds(pl.multiple_of(tp * 16, 16), rows)].astype(F32)
     seam_in = [product_in[:16].astype(F32)[15:], product_in[rows:].astype(F32)[:1]]
 
-    @pl.when(((tp == 0) & has_left) | ((tp == 1) & has_right))
-    def _():
-        for q in range(tp_size):
-            wait_for(edge_in.at[q], edge_recv.at[q, 0])
-            wait_for(doc_in.at[q], edge_recv.at[q, 1])
-
     doc = jnp.broadcast_to(docs[...], (8, length))
-    beyond = jnp.broadcast_to(doc_in[0], (8, length))
     lane = lax.broadcasted_iota(jnp.int32, (8, length), 1)
-    prior = pltpu.roll(jnp.where(lane == length - 1, beyond, doc), 1, axis=1)
-    later = pltpu.roll(jnp.where(lane == 0, beyond, doc), length - 1, axis=1)
-    spot = lane + sp * length
-    same_prev = jnp.where((prior == doc) & (spot > 0), 1.0, 0.0)
-    same_next = jnp.where((later == doc) & (spot < sp_size * length - 1), 1.0, 0.0)
+    same_prev = jnp.where((pltpu.roll(doc, 1, axis=1) == doc) & (lane > 0), 1.0, 0.0)
+    same_next = jnp.where(
+        (pltpu.roll(doc, length - 1, axis=1) == doc) & (lane < length - 1), 1.0, 0.0
+    )
 
     def column(row):
         mine = jnp.where(tp == 0, row[:1, :rows], row[:1, rows:])
@@ -320,50 +312,69 @@
 
     before_col, after_col = column(same_prev), column(same_next)
 
-    def mix(values_f, ends, edge, weights, gate):
-        first = jnp.where(tp == 0, edge[15:], ends[0])
-        last = jnp.where(tp == 0, ends[1], edge[:1])
-        prev = jnp.where(row_at == 0, first, pltpu.roll(values_f, 1, axis=0))
-        nxt = jnp.where(row_at == rows - 1, last, pltpu.roll(values_f, rows - 1, axis=0))
-        conv = (
+    def convolve(values_f, ends, weights):
+        prev = jnp.where(row_at == 0, ends[0], pltpu.roll(values_f, 1, axis=0))
+        nxt = jnp.where(row_at == rows - 1, ends[1], pltpu.roll(values_f, rows - 1, axis=0))
+        return (
             weights[0:1] * prev * before_col
             + weights[1:2] * values_f
             + weights[2:3] * nxt * after_col
         )
-        return (gate.astype(F32) * conv).astype(BF16)
-
-    mine = mix(
-        prod, seam, edge_in[tp].astype(F32), taps[...],
-        outer[pl.ds(pl.multiple_of(tp * rows, rows), rows)],
-    )
-    theirs = mix(prod_in, seam_in, edge_in[other].astype(F32), taps_in[...], outer_in[...])
+
+    halves = [
+        (
+            convolve(prod, seam, taps[...]), taps,
+            outer[pl.ds(pl.multiple_of(tp * rows, rows), rows)].astype(F32), tp,
+        ),
+        (convolve(prod_in, seam_in, taps_in[...]), taps_in, outer_in[...].astype(F32), other),
+    ]
+    mixed = [(gate * conv).astype(BF16) for conv, _, gate, _ in halves]
     loads[3].wait()
     loads[4].wait()
+
+    def project(pieces, c):
+        return sum(
+            dot(piece, ow[pl.ds(pl.multiple_of(half[3] * chan, chan), chan), c * tile : (c + 1) * tile])
+            for piece, half in zip(pieces, halves)
+        )
+
     squares = jnp.zeros((rows, 1), F32)
     for c in range(PARTS):
-        cols = slice(c * tile, (c + 1) * tile)
-        part = (
-            stream[:, cols].astype(F32)
-            + dot(mine, ow[pl.ds(pl.multiple_of(tp * chan, chan), chan), cols])
-            + dot(theirs, ow[pl.ds(pl.multiple_of(other * chan, chan), chan), cols])
-        )
+        part = stream[:, c * tile : (c + 1) * tile].astype(F32) + project(mixed, c)
         resid[c] = part
         squares = squares + jnp.sum(part * part, axis=1, keepdims=True)
     scale = lax.rsqrt(squares / width + 1e-06)
 
+    def first_rows(x):
+        return jnp.where(tp == 0, x[:16], x[rows - 16 :])
+
+    late = pl.ds(pl.multiple_of(tp * (rows - 16), 16), 16)
+    early = pl.ds(pl.multiple_of(other * 16, 16), rows - 16)
+
     def hop(j, c, sem, device):
         return remote(block.at[j, c], block.at[j, c], sem, hop_recv.at[j, c], device)
 
-    def own_in(c):
-        return hop(z, c, in_send.at[0, c], inward)
-
-    def own_out(c):
-        return hop(z, c, out_send.at[0, c], outward)
+    def own(c, which, sem, device):
+        ref = block.at[z, c, which]
+        return remote(ref, ref, sem, hop_recv.at[z, c], device)
+
+    def own_start(c, which):
+        @pl.when(is_middle)
+        def _():
+            own(c, which, out_send, outward).start()
+
+        if c < 2:
+            own(c, which, in_send, inward).start()
+        else:
+
+            @pl.when(is_end)
+            def _():
+                own(c, which, in_send, inward).start()
 
     def onward(i, c):
         if i == 1:
-            return hop(order[1], c, in_send.at[1, c], inward)
-        return hop(order[i], c, out_send.at[i - 1, c], outward)
+            return hop(order[1], c, in_send, inward)
+        return hop(order[i], c, out_send, outward)
 
     def forward(i, c):
         wait_for(block.at[order[i], c], hop_recv.at[order[i], c])
@@ -388,7 +399,7 @@
         send[i, c] = (
             dot(picks[i], block[order[i], c]).astype(BF16).reshape(per_plane, cap, tile)
         )
-        group(send.at[i, c], recv.at[i, c], disp_send.at[i, c], disp_recv.at[i, c])
+        group(send.at[i, c], recv.at[i, c], disp_send, disp_recv.at[i, c])
         recv[i, c, p] = send[i, c, p]
 
     def upward(i, c):
@@ -406,22 +417,25 @@
             else:
                 hidden[:, f : f + 256] = (a / (1.0 + jnp.exp(-a)) * b).astype(BF16)
 
-    def downward(i):
-        for c in range(PARTS):
-            outb[i, c] = (
-                dot(hidden[...], wd[:, c * tile : (c + 1) * tile])
-                .astype(BF16)
-                .reshape(per_plane, cap, tile)
-            )
-            group(outb.at[i, c], ret.at[i, c], back_send.at[i, c], back_recv.at[i, c])
-            ret[i, c, p] = outb[i, c, p]
+    def hand_back(i, c):
+        group(outb.at[i, c], ret.at[i, c], back_send, back_recv.at[i, c])
+
+    def downward(i, c, sends):
+        outb[i, c] = (
+            dot(hidden[...], wd[:, c * tile : (c + 1) * tile])
+            .astype(BF16)
+            .reshape(per_plane, cap, tile)
+        )
+        if sends:
+            hand_back(i, c)
+        ret[i, c, p] = outb[i, c, p]
 
     spread_back, relaying = {}, [False]
 
     def part_copy(i, c, slot, device):
         return remote(
             part_out.at[i - 1, c], part_in.at[slot, c],
-            part_send.at[i - 1, c], part_recv.at[slot, c], device,
+            part_send, part_recv.at[slot, c], device,
         )
 
     def combine(i, c):
@@ -459,23 +473,48 @@
         result[c] = (part + part_in[z, c].astype(F32)).astype(BF16)
         deliver(c).start()
 
+    def normed(part, by, c):
+        return (part * by * gain[:, c * tile : (c + 1) * tile]).astype(BF16)
+
     for c in range(PARTS):
-        block[z, c] = (
-            resid[c] * scale * gain[:, c * tile : (c + 1) * tile]
-        ).astype(BF16)
-
+        block[z, c] = normed(resid[c], scale, c)
         if c < 2:
-            own_in(c).start()
-        else:
-
-            @pl.when(is_end)
-            def _():
-                own_in(c).start()
-
-        @pl.when(is_middle)
-        def _():
-            own_out(c).start()
-
+            own_start(c, early)
+
+    @pl.when(((tp == 0) & has_left) | ((tp == 1) & has_right))
+    def _():
+        for q in range(tp_size):
+            wait_for(edge_in.at[q], edge_recv.at[q, 0])
+            wait_for(doc_in.at[q], edge_recv.at[q, 1])
+
+    ours = jnp.where(tp == 0, docs[:, :1], docs[:, length - 1 :])
+    beyond = jnp.where(tp == 0, doc_in[0][:, length - 1 :], doc_in[0][:, :1])
+    inside = jnp.where(tp == 0, sp > 0, sp < sp_size - 1)
+    joined = jnp.where((ours == beyond) & inside, 1.0, 0.0)
+    at_edge = lax.broadcasted_iota(jnp.int32, (16, chan), 0) == tp * 15
+    fixed = []
+    for conv, weights, gate, half in halves:
+        edge = edge_in[half].astype(F32)
+        term = (
+            jnp.where(tp == 0, weights[0:1], weights[2:3])
+            * jnp.where(tp == 0, edge[15:], edge[:1])
+            * joined
+        )
+        fixed.append(
+            (first_rows(gate) * (first_rows(conv) + jnp.where(at_edge, term, 0.0))).astype(BF16)
+        )
+    squares = jnp.zeros((16, 1), F32)
+    parts = []
+    for c in range(PARTS):
+        part = stream[late, c * tile : (c + 1) * tile].astype(F32) + project(fixed, c)
+        resid[c, late] = part
+        parts.append(part)
+        squares = squares + jnp.sum(part * part, axis=1, keepdims=True)
+    late_scale = lax.rsqrt(squares / width + 1e-06)
+    for c in range(PARTS):
+        block[z, c, late] = normed(parts[c], late_scale, c)
+        own_start(c, late if c < 2 else pl.ds(0, rows))
+    for c in range(PARTS):
         dispatch(0, c)
 
     for i in range(1, planes):
@@ -485,7 +524,7 @@
 
     def own_rest():
         for c in range(2, PARTS):
-            own_in(c).start()
+            hop(z, c, in_send, inward).start()
 
     def run(plan, relays):
         relaying[0] = relays
@@ -494,7 +533,9 @@
         steps = {
             "U": upward, "D": dispatch, "F": forward, "C": combine, "R": relay,
             "E": lambda i, c: finish(c, i == 1),
-            "N": lambda i, c: downward(i),
+            "N": lambda i, c: downward(i, c, True),
+            "K": lambda i, c: downward(i, c, False),
+            "S": hand_back,
             "P": lambda i, c: picks.append(to_slots(i)),
             "W": lambda i, c: loads[7].wait(),
             "O": lambda i, c: own_rest(),
@@ -506,10 +547,11 @@
     def _():
         run(
             (
-                "U00 U01 U02 P10", "D10 U03 W00 N00", "D11 D12 C00 U10", "D13 U11 C01 C02",
-                "C03 U12 P20 D20", "U13 D21 N10 U20", "D22 U21 C10 D23", "C11 C12 P30 D30",
-                "C13 U22 D31 U23", "N20 D32 U30 U31", "C20 D33 C21 C22", "C23 U32 U33 N30",
-                "C30 C31 C32 C33", "E00 E01 E02 E03",
+                "U00 P10 D10 D11", "U01 D12 U02 U03", "W00 K00 K01 K02", "K03 D13 S00 U10",
+                "U11 U12 U13 N10", "N11 N12 P20 D20", "N13 C10 P30 D21", "C11 C12 U20 D22",
+                "C13 U21 D23 U22", "D30 D31 U23 N20", "D32 N21 U30 D33", "N22 C20 N23 C21",
+                "U31 U32 C22 U33", "N30 N31 N32 N33", "S01 S02 S03 C23", "C30 C31 C32 C33",
+                "C00 C01 C02 C03", "E00 E01 E02 E03",
             ),
             False,
         )
@@ -518,11 +560,12 @@
     def _():
         run(
             (
-                "P10 U00 F10 D10", "U01 U02 F11 D11", "U03 W00 N00 F12", "D12 P20 F20 D20",
-                "F13 O00 D13 F21", "D21 U10 U11 C00", "C01 F22 D22 C02", "C03 F23 D23 U12",
-                "P30 U13 N10 F30", "F31 D30 D31 U20", "U21 F32 D32 U22", "U23 F33 D33 N20",
-                "C10 C11 C12 C13", "U30 U31 U32 U33", "N30 C20 C21 R20", "C22 C23 R21 C30",
-                "R10 C31 R22 C32", "R11 C33 R23 R12", "R30 R13 R31 R32", "E10 R33 E11 E12", "E13",
+                "P10 U00 F10 D10", "F11 D11 U01 U02", "F12 D12 F30 P20", "U03 W00 K00 K01",
+                "K02 K03 F13 O00", "D13 F20 D20 U10", "U11 F21 D21 U12", "U13 F22 D22 N10",
+                "N11 N12 N13 F23", "D23 F31 P30 D30", "D31 U20 U21 F32", "D32 C10 C11 U22",
+                "F33 D33 C12 C13", "U23 N20 N21 N22", "N23 U30 U31 U32", "U33 N30 N31 N32",
+                "N33 S00 S01 S02", "S03 C20 R20 C21", "R21 C22 C23 R22", "C30 R10 C31 R23",
+                "C32 R11 C33 R12", "C00 R30 R13 C01", "R31 C02 R32 C03", "E10 R33 E11 E12", "E13",
             ),
             True,
         )
@@ -540,20 +583,19 @@
         for copy in to_left:
             copy.wait_send()
 
-    for c in range(PARTS):
-        own_in(c).wait_send()
-        for i in range(planes):
-            wait_group(send.at[i, c], disp_send.at[i, c])
-            wait_group(outb.at[i, c], back_send.at[i, c])
-        for i in range(1, planes):
-            wait_for(part_out.at[i - 1, c], part_send.at[i - 1, c])
+    most = pl.ds(0, per_plane - 1)
+    wait_for(send.at[:, :, most], disp_send)
+    wait_for(outb.at[:, :, most], back_send)
+    wait_for(part_out, part_send)
+
+    @pl.when(is_end)
+    def _():
+        wait_for(block.at[0], in_send)
 
     @pl.when(is_middle)
     def _():
-        for c in range(PARTS):
-            own_out(c).wait_send()
-            for i in range(1, planes):
-                onward(i, c).wait_send()
+        wait_for(block.at[pl.ds(0, 2)], in_send)
+        wait_for(block.at[pl.ds(0, 3)], out_send)
 
     for c in range(PARTS):
         deliver(c).wait()
@@ -605,10 +647,8 @@
             pltpu.VMEM((planes - 1, PARTS, rows, tile), BF16),
             pltpu.VMEM((planes + 1, PARTS, rows, tile), BF16),
             dma((8,)), dma((4,)), dma((2, 2)), dma((3,)), dma((3,)), dma((planes - 1,)), dma((planes,)),
-            dma((2, PARTS)), dma((3, PARTS)), dma((planes, PARTS)),
-            dma((planes, PARTS)), dma((planes, PARTS)),
-            dma((planes, PARTS)), dma((planes, PARTS)),
-            dma((planes - 1, PARTS)), dma((planes + 1, PARTS)), dma((PARTS,)),
+            dma, dma, dma((planes, PARTS)), dma, dma((planes, PARTS)), dma, dma((planes, PARTS)),
+            dma, dma((planes + 1, PARTS)), dma((PARTS,)),
         ],
         compiler_params=pltpu.CompilerParams(
             collective_id=0, has_side_effects=True, vmem_limit_bytes=56 * 1024 * 1024

time: 81 us -> 77.2 us (0.953)
  Pallas kernels: 78.9 us -> 75.1 us
    pallas_call x1, Pallas kernels: 78.9 us -> 75.1 us  [fused(): pl.pallas_call(functools.partial(fused_kernel, tp_size, planes, per_plane...]
where the time goes in v3:
time: 77.2 us; the launch traced here: 77 us
  Pallas kernels  75.1 us (97%)
  local copies, waits for them, and re-layouts  1.88 us (2%)
    pallas_call x1, Pallas kernels, fused(): pl.pallas_call(functools.partial(fused_kernel, tp_size, planes, per_plane...  75.1 us
    unnamed x1, local copies, waits for them, and re-layouts  1.88 us

profile of v3, /device:TPU:8, one launch (start us, length us, event | category | flops | bytes accessed | tf_op | source)
XLA Modules:
  0.0 77.0 jit_solution(8977025248538336774)
XLA Ops:
  0.0 75.1 %shard_map.136 = bf16[128,2048]{1,0:T(8,128)(2,1)} custom-call(s32[1,256]{1,0:T(1,128)} %bitcast.6, f32[3,512]{1,0:T(4,128)} %taps.1, f32[1,2048]{1,0:T(1,128)} %bitcast.5, s32[2,128]{1,0:T(2,128)} %bitcast.7, f32[2,128]{1,0:T(2,128)} %bitcast.8, f32[1,128]{1,0:T(1,128)} %bitcast.9, bf16[256,512]{1,0:T(8,128)(2,1)} %inner_hbm.1, ...), custom_call_target="tpu_custom_call" | custom-call | tf_op jit(solution)/shard_map/pallas_call | solution.py:617
  75.1 1.9 %copy.16 = bf16[128,2048]{1,0:T(8,128)(2,1)} copy(bf16[128,2048]{1,0:T(8,128)(2,1)} %shard_map.136) | data formatting | bytes 1048576

commit v4 on v3

--- a/solution.py
+++ b/solution.py
@@ -115,15 +115,15 @@
 
 def fused_kernel(
     tp_size, planes, per_plane, cap,
-    docs, taps, gain, ids, logits, weight,
-    inner_hbm, values_hbm, outer_hbm, stream_hbm, ow_hbm, wg_hbm, wu_hbm, wd_hbm,
+    inner_hbm, values_hbm, ids_hbm, logits_hbm, weight_hbm, docs_hbm, taps_hbm, outer_hbm,
+    gain_hbm, stream_hbm, ow_hbm, wg_hbm, wu_hbm, wd_hbm,
     out,
-    inner, values, outer, stream, ow, wg, wu, wd,
-    product, product_in, outer_in, taps_in, edge_out, edge_in, doc_in, resid, result,
+    inner, values, ids, logits, weight, docs, taps, outer, gain, stream, ow, wg, wu, wd,
+    product, product_in, outer_in, taps_in, edge_out, edge_in, doc_in, resid,
     meta, block, send, recv, outb, ret, acc_gate, acc_up, hidden, local, part_out, part_in,
     load_sem, edge_send, edge_recv, swap_send, swap_recv, meta_send, meta_recv,
     in_send, out_send, hop_recv, disp_send, disp_recv, back_send, back_recv,
-    part_send, part_recv, result_sem,
+    part_send, part_recv,
 ):
     sp, tp = lax.axis_index("sp"), lax.axis_index("tp")
     sp_size = planes * per_plane // tp_size
@@ -161,8 +161,9 @@
         pltpu.make_async_copy(src, dst, load_sem.at[i])
         for i, (src, dst) in enumerate(
             (
-                (inner_hbm, inner), (values_hbm, values), (outer_hbm, outer),
-                (stream_hbm, stream), (ow_hbm, ow),
+                (inner_hbm, inner), (values_hbm, values), (ids_hbm, ids), (logits_hbm, logits),
+                (weight_hbm, weight), (docs_hbm, docs), (taps_hbm, taps), (outer_hbm, outer),
+                (gain_hbm, gain), (stream_hbm, stream), (ow_hbm, ow),
                 (wg_hbm.at[0], wg), (wu_hbm.at[0], wu), (wd_hbm.at[0], wd),
             )
         )
@@ -190,10 +191,6 @@
         greet(place((z + d) % planes * per_plane + p))
     for d in range(1, per_plane):
         greet(place(z * per_plane + (p + d) % per_plane))
-
-    expo = jnp.exp(logits[...])
-    gates = weight[...] * expo / jnp.sum(expo, axis=0, keepdims=True)
-    meta[z] = jnp.concatenate([ids[...].astype(F32), gates, ids[...].astype(F32), gates], axis=0)
 
     @pl.when(((tp == 0) & (sp == 0)) | ((tp == 1) & (sp == sp_size - 1)))
     def _():
@@ -205,7 +202,11 @@
     product[...] = (inner[...].astype(F32) * values[...].astype(F32)).astype(BF16)
     edge_out[0] = product[:16]
     edge_out[1] = product[length - 16 :]
-    loads[2].wait()
+    for load in loads[2:8]:
+        load.wait()
+    expo = jnp.exp(logits[...])
+    gates = weight[...] * expo / jnp.sum(expo, axis=0, keepdims=True)
+    meta[z] = jnp.concatenate([ids[...].astype(F32), gates, ids[...].astype(F32), gates], axis=0)
     pl.semaphore_wait(
         barrier,
         planes + per_plane - 2 + (sp + sp_size - 1) // sp_size + (2 * sp_size - 2 - sp) // sp_size,
@@ -329,13 +330,16 @@
         (convolve(prod_in, seam_in, taps_in[...]), taps_in, outer_in[...].astype(F32), other),
     ]
     mixed = [(gate * conv).astype(BF16) for conv, _, gate, _ in halves]
-    loads[3].wait()
-    loads[4].wait()
+    for load in loads[8:11]:
+        load.wait()
 
     def project(pieces, c):
         return sum(
-            dot(piece, ow[pl.ds(pl.multiple_of(half[3] * chan, chan), chan), c * tile : (c + 1) * tile])
-            for piece, half in zip(pieces, halves)
+            dot(
+                rows_of,
+                ow[pl.ds(pl.multiple_of(half[3] * chan, chan), chan), c * tile : (c + 1) * tile],
+            )
+            for rows_of, half in zip(pieces, halves)
         )
 
     squares = jnp.zeros((rows, 1), F32)
@@ -351,51 +355,56 @@
     late = pl.ds(pl.multiple_of(tp * (rows - 16), 16), 16)
     early = pl.ds(pl.multiple_of(other * 16, 16), rows - 16)
 
-    def hop(j, c, sem, device):
-        return remote(block.at[j, c], block.at[j, c], sem, hop_recv.at[j, c], device)
-
-    def own(c, which, sem, device):
-        ref = block.at[z, c, which]
-        return remote(ref, ref, sem, hop_recv.at[z, c], device)
-
-    def own_start(c, which):
+    def piece(j, n):
+        if n == PARTS:
+            return block.at[j, pl.ds(0, 2), late]
+        return block.at[j, n, early] if n < 2 else block.at[j, n]
+
+    def hop(j, n, sem, device):
+        return remote(piece(j, n), piece(j, n), sem, hop_recv.at[j, n], device)
+
+    def own_start(n):
         @pl.when(is_middle)
         def _():
-            own(c, which, out_send, outward).start()
-
-        if c < 2:
-            own(c, which, in_send, inward).start()
+            hop(z, n, out_send, outward).start()
+
+        if n < 2 or n == PARTS:
+            hop(z, n, in_send, inward).start()
         else:
 
             @pl.when(is_end)
             def _():
-                own(c, which, in_send, inward).start()
-
-    def onward(i, c):
+                hop(z, n, in_send, inward).start()
+
+    def arrived(i, n):
+        wait_for(piece(order[i], n), hop_recv.at[order[i], n])
+
+    def forward(i, n):
+        arrived(i, n)
         if i == 1:
-            return hop(order[1], c, in_send, inward)
-        return hop(order[i], c, out_send, outward)
-
-    def forward(i, c):
-        wait_for(block.at[order[i], c], hop_recv.at[order[i], c])
-        onward(i, c).start()
+            hop(order[1], n, in_send, inward).start()
+        else:
+            hop(order[i], n, out_send, outward).start()
+
+    peers = [
+        (p // 4 + k // 4) % 2 * 4 + (p // 2 + k // 2) % 2 * 2 + (p + k) % 2
+        for k in range(per_plane - 1, 0, -1)
+    ]
 
     def group(src, dst, source_sem, target_sem):
-        def one(i, carry):
-            peer = (p + i) % per_plane
+        for peer in peers:
             remote(
                 src.at[peer], dst.at[p], source_sem, target_sem, place(z * per_plane + peer)
             ).start()
-            return carry
-
-        lax.fori_loop(1, per_plane, one, 0)
 
     def wait_group(buf, sem):
         wait_for(buf.at[pl.ds(0, per_plane - 1)], sem)
 
     def dispatch(i, c):
         if i > 0 and not relaying[0]:
-            wait_for(block.at[order[i], c], hop_recv.at[order[i], c])
+            arrived(i, c)
+            if c == 0:
+                arrived(i, PARTS)
         send[i, c] = (
             dot(picks[i], block[order[i], c]).astype(BF16).reshape(per_plane, cap, tile)
         )
@@ -459,19 +468,13 @@
         part_out[i - 1, c] = (local[i - 1, c] + part_in[order[i], c].astype(F32)).astype(BF16)
         part_copy(i, c, order[i], outward if i == 1 else inward).start()
 
-    def deliver(c):
-        return pltpu.make_async_copy(
-            result.at[c], out.at[:, pl.ds(c * tile, tile)], result_sem.at[c]
-        )
-
     def finish(c, both):
         part = resid[c]
         if both:
             wait_for(part_in.at[planes, c], part_recv.at[planes, c])
             part = part + part_in[planes, c].astype(F32)
         wait_for(part_in.at[z, c], part_recv.at[z, c])
-        result[c] = (part + part_in[z, c].astype(F32)).astype(BF16)
-        deliver(c).start()
+        out[:, c * tile : (c + 1) * tile] = (part + part_in[z, c].astype(F32)).astype(BF16)
 
     def normed(part, by, c):
         return (part * by * gain[:, c * tile : (c + 1) * tile]).astype(BF16)
@@ -479,7 +482,7 @@
     for c in range(PARTS):
         block[z, c] = normed(resid[c], scale, c)
         if c < 2:
-            own_start(c, early)
+            own_start(c)
 
     @pl.when(((tp == 0) & has_left) | ((tp == 1) & has_right))
     def _():
@@ -513,13 +516,14 @@
     late_scale = lax.rsqrt(squares / width + 1e-06)
     for c in range(PARTS):
         block[z, c, late] = normed(parts[c], late_scale, c)
-        own_start(c, late if c < 2 else pl.ds(0, rows))
+        if c > 0:
+            own_start(c if c > 1 else PARTS)
     for c in range(PARTS):
         dispatch(0, c)
 
     for i in range(1, planes):
         wait_for(meta.at[order[i]], meta_recv.at[order[i]])
-    for load in loads[5:7]:
+    for load in loads[11:13]:
         load.wait()
 
     def own_rest():
@@ -537,7 +541,7 @@
             "K": lambda i, c: downward(i, c, False),
             "S": hand_back,
             "P": lambda i, c: picks.append(to_slots(i)),
-            "W": lambda i, c: loads[7].wait(),
+            "W": lambda i, c: loads[13].wait(),
             "O": lambda i, c: own_rest(),
         }
         for name in " ".join(plan).split():
@@ -547,10 +551,10 @@
     def _():
         run(
             (
-                "U00 P10 D10 D11", "U01 D12 U02 U03", "W00 K00 K01 K02", "K03 D13 S00 U10",
-                "U11 U12 U13 N10", "N11 N12 P20 D20", "N13 C10 P30 D21", "C11 C12 U20 D22",
-                "C13 U21 D23 U22", "D30 D31 U23 N20", "D32 N21 U30 D33", "N22 C20 N23 C21",
-                "U31 U32 C22 U33", "N30 N31 N32 N33", "S01 S02 S03 C23", "C30 C31 C32 C33",
+                "U00 P10 D10 D11", "U01 D12 U02 U03", "W00 K00 K01 K02", "K03 D13 S00 S01",
+                "U10 U11 U12 U13", "N10 N11 P20 D20", "D21 C10 D22 N12", "C11 D23 N13 U20",
+                "U21 C12 U22 P30", "U23 N20 D30 D31", "C13 N21 D32 C20", "N22 D33 N23 C21",
+                "U30 U31 C22 U32", "U33 N30 N31 N32", "N33 S02 S03 C23", "C30 C31 C32 C33",
                 "C00 C01 C02 C03", "E00 E01 E02 E03",
             ),
             False,
@@ -560,12 +564,13 @@
     def _():
         run(
             (
-                "P10 U00 F10 D10", "F11 D11 U01 U02", "F12 D12 F30 P20", "U03 W00 K00 K01",
-                "K02 K03 F13 O00", "D13 F20 D20 U10", "U11 F21 D21 U12", "U13 F22 D22 N10",
-                "N11 N12 N13 F23", "D23 F31 P30 D30", "D31 U20 U21 F32", "D32 C10 C11 U22",
-                "F33 D33 C12 C13", "U23 N20 N21 N22", "N23 U30 U31 U32", "U33 N30 N31 N32",
-                "N33 S00 S01 S02", "S03 C20 R20 C21", "R21 C22 C23 R22", "C30 R10 C31 R23",
-                "C32 R11 C33 R12", "C00 R30 R13 C01", "R31 C02 R32 C03", "E10 R33 E11 E12", "E13",
+                "P10 F10 U00 F11", "F14 D10 D11 U01", "U02 F20 F12 D12", "P20 U03 W00 K00",
+                "K01 K02 K03 F21", "F24 D20 D21 F13", "O00 D13 U10 U11", "F22 D22 U12 F23",
+                "D23 U13 N10 N11", "N12 N13 F30 F31", "F34 U20 U21 U22", "U23 N20 N21 N22",
+                "N23 F32 F33 P30", "D30 D31 D32 D33", "C10 C11 C12 C13", "C20 C21 U30 U31",
+                "C22 C23 U32 U33", "N30 N31 N32 N33", "R20 R21 S00 S01", "S02 S03 R22 C30",
+                "R10 C31 R23 C32", "R11 C33 R12 C00", "R30 R13 C01 R31", "C02 R32 C03 E10",
+                "R33 E11 E12 E13",
             ),
             True,
         )
@@ -596,9 +601,6 @@
     def _():
         wait_for(block.at[pl.ds(0, 2)], in_send)
         wait_for(block.at[pl.ds(0, 3)], out_send)
-
-    for c in range(PARTS):
-        deliver(c).wait()
 
 
 def fused(
@@ -608,21 +610,25 @@
 ):
     rows, width = stream.shape
     length, chan = inner_gate.shape
-    ff = w_gate.shape[2]
+    ff, top = w_gate.shape[2], route_ids.shape[1]
     tile = width // PARTS
-    vmem = pl.BlockSpec(memory_space=pltpu.VMEM)
-    anywhere = pl.BlockSpec(memory_space=pl.ANY)
     slotted = pltpu.VMEM((planes, PARTS, per_plane, cap, tile), BF16)
     dma = pltpu.SemaphoreType.DMA
     return pl.pallas_call(
         functools.partial(fused_kernel, tp_size, planes, per_plane, cap),
         out_shape=jax.ShapeDtypeStruct((rows, width), BF16),
-        in_specs=[vmem] * 6 + [anywhere] * 8,
-        out_specs=anywhere,
+        in_specs=[pl.BlockSpec(memory_space=pltpu.HBM)] * 14,
+        out_specs=pl.BlockSpec(memory_space=pltpu.VMEM),
         scratch_shapes=[
             pltpu.VMEM((length, chan), BF16),
             pltpu.VMEM((length, chan), BF16),
+            pltpu.VMEM((top, rows), jnp.int32),
+            pltpu.VMEM((top, rows), F32),
+            pltpu.VMEM((1, rows), F32),
+            pltpu.VMEM((1, length), jnp.int32),
+            pltpu.VMEM(conv_taps.shape, F32),
             pltpu.VMEM((length, chan), BF16),
+            pltpu.VMEM((1, width), F32),
             pltpu.VMEM((rows, width), BF16),
             pltpu.VMEM(out_weight.shape, BF16),
             pltpu.VMEM((width, ff), BF16),
@@ -636,7 +642,6 @@
             pltpu.VMEM((2, 16, chan), BF16),
             pltpu.VMEM((2, 1, length), jnp.int32),
             pltpu.VMEM((PARTS, rows, tile), F32),
-            pltpu.VMEM((PARTS, rows, tile), BF16),
             pltpu.VMEM((planes, 8, rows), F32),
             pltpu.VMEM((planes, PARTS, rows, tile), BF16),
             slotted, slotted, slotted, slotted,
@@ -646,17 +651,22 @@
             pltpu.VMEM((planes - 1, PARTS, rows, tile), F32),
             pltpu.VMEM((planes - 1, PARTS, rows, tile), BF16),
             pltpu.VMEM((planes + 1, PARTS, rows, tile), BF16),
-            dma((8,)), dma((4,)), dma((2, 2)), dma((3,)), dma((3,)), dma((planes - 1,)), dma((planes,)),
-            dma, dma, dma((planes, PARTS)), dma, dma((planes, PARTS)), dma, dma((planes, PARTS)),
-            dma, dma((planes + 1, PARTS)), dma((PARTS,)),
+            dma((14,)), dma((4,)), dma((2, 2)), dma((3,)), dma((3,)), dma((planes - 1,)), dma((planes,)),
+            dma, dma, dma((planes, PARTS + 1)), dma, dma((planes, PARTS)), dma, dma((planes, PARTS)),
+            dma, dma((planes + 1, PARTS)),
         ],
         compiler_params=pltpu.CompilerParams(
-            collective_id=0, has_side_effects=True, vmem_limit_bytes=56 * 1024 * 1024
+            collective_id=0, has_side_effects=True, vmem_limit_bytes=48 * 1024 * 1024
         ),
     )(
-        doc_ids[None, :], conv_taps, norm_gain[None, :],
-        route_ids.T, route_logits.T, group_weight[None, :],
-        inner_gate, conv_values, outer_gate, stream, out_weight, w_gate, w_up, w_down,
+        *[
+            pltpu.with_memory_space_constraint(x, pltpu.HBM)
+            for x in (
+                inner_gate, conv_values, route_ids.T, route_logits.T, group_weight[None, :],
+                doc_ids[None, :], conv_taps, outer_gate, norm_gain[None, :], stream,
+                out_weight, w_gate, w_up, w_down,
+            )
+        ]
     )
 
 
@@ -668,7 +678,7 @@
     cap = 2 * stream.shape[0] * top // total
     planes = 4
     per_plane = total // planes
-    if tp_size != 2 or top != 2 or total % planes or cap % 16 or per_plane * cap != stream.shape[0]:
+    if tp_size != 2 or top != 2 or per_plane != 8 or total % planes or cap % 16 or per_plane * cap != stream.shape[0]:
         return on_device(*args)
     return fused(tp_size, planes, per_plane, cap, *args)
 

time: 77.2 us -> 74 us (0.959)
  Pallas kernels: 75.1 us -> 73.1 us
  local copies, waits for them, and re-layouts: 1.88 us -> 0.8 us
    pallas_call x1, Pallas kernels: 75.1 us -> 73.1 us  [fused(): pl.pallas_call(functools.partial(fused_kernel, tp_size, planes, per_plane...]
    unnamed x1, local copies, waits for them, and re-layouts: 1.88 us -> 0.8 us
where the time goes in v4:
time: 74 us; the launch traced here: 73.9 us
  Pallas kernels  73.1 us (99%)
  local copies, waits for them, and re-layouts  0.8 us (1%)
    pallas_call x1, Pallas kernels, fused(): pl.pallas_call(functools.partial(fused_kernel, tp_size, planes, per_plane...  73.1 us

profile of v4, /device:TPU:8, one launch (start us, length us, event | category | flops | bytes accessed | tf_op | source)
XLA Modules:
  0.0 73.9 jit_solution(10092452114921531788)
XLA Ops:
  0.0 73.1 %shard_map.136 = bf16[128,2048]{1,0:T(8,128)(2,1)S(1)} custom-call(bf16[256,512]{1,0:T(8,128)(2,1)} %inner_hbm.1, bf16[256,512]{1,0:T(8,128)(2,1)} %values_hbm.1, s32[2,128]{1,0:T(2,128)} %bitcast.6, f32[2,128]{1,0:T(2,128)} %bitcast.7, f32[1,128]{1,0:T(1,128)} %bitcast.9, s32[1,256]{1,0:T(1,128)} %bitcast.8, f32[3,512]{1,0:T(4,128)} %taps_hbm.1, ...), custom_call_target="tpu_custom_call" | custom-call | tf_op jit(solution)/shard_map/pallas_call | solution.py:617
  73.1 0.8 %copy.16 = bf16[128,2048]{1,0:T(8,128)(2,1)} copy(bf16[128,2048]{1,0:T(8,128)(2,1)S(1)} %shard_map.136) | data formatting | bytes 1048576

commit v5 on v4

--- a/solution.py
+++ b/solution.py
@@ -441,10 +441,15 @@
 
     spread_back, relaying = {}, [False]
 
-    def part_copy(i, c, slot, device):
+    def halves_of(i, c):
+        if i == planes - 1 and c == PARTS - 1:
+            return [(pl.ds(0, rows // 2), c), (pl.ds(rows // 2, rows // 2), PARTS)]
+        return [(pl.ds(0, rows), c)]
+
+    def part_copy(i, c, slot, device, span, sem):
         return remote(
-            part_out.at[i - 1, c], part_in.at[slot, c],
-            part_send, part_recv.at[slot, c], device,
+            part_out.at[i - 1, c, span], part_in.at[slot, c, span],
+            part_send, part_recv.at[slot, sem], device,
         )
 
     def combine(i, c):
@@ -461,19 +466,24 @@
             local[i - 1, c] = part
         else:
             part_out[i - 1, c] = part.astype(BF16)
-            part_copy(i, c, planes if i == 1 else order[i], inward).start()
+            for span, sem in halves_of(i, c):
+                part_copy(i, c, planes if i == 1 else order[i], inward, span, sem).start()
 
     def relay(i, c):
-        wait_for(part_in.at[order[i], c], part_recv.at[order[i], c])
-        part_out[i - 1, c] = (local[i - 1, c] + part_in[order[i], c].astype(F32)).astype(BF16)
-        part_copy(i, c, order[i], outward if i == 1 else inward).start()
+        for span, sem in halves_of(i, c):
+            wait_for(part_in.at[order[i], c, span], part_recv.at[order[i], sem])
+            part_out[i - 1, c, span] = (
+                local[i - 1, c, span] + part_in[order[i], c, span].astype(F32)
+            ).astype(BF16)
+            part_copy(i, c, order[i], outward if i == 1 else inward, span, sem).start()
 
     def finish(c, both):
         part = resid[c]
         if both:
             wait_for(part_in.at[planes, c], part_recv.at[planes, c])
             part = part + part_in[planes, c].astype(F32)
-        wait_for(part_in.at[z, c], part_recv.at[z, c])
+        for span, sem in halves_of(planes - 1 if both else 1, c):
+            wait_for(part_in.at[z, c, span], part_recv.at[z, sem])
         out[:, c * tile : (c + 1) * tile] = (part + part_in[z, c].astype(F32)).astype(BF16)
 
     def normed(part, by, c):
@@ -552,8 +562,8 @@
         run(
             (
                 "U00 P10 D10 D11", "U01 D12 U02 U03", "W00 K00 K01 K02", "K03 D13 S00 S01",
-                "U10 U11 U12 U13", "N10 N11 P20 D20", "D21 C10 D22 N12", "C11 D23 N13 U20",
-                "U21 C12 U22 P30", "U23 N20 D30 D31", "C13 N21 D32 C20", "N22 D33 N23 C21",
+                "U10 U11 U12 U13", "N10 N11 P20 D20", "D21 C10 D22 C11", "D23 N12 N13 U20",
+                "U21 U22 P30 U23", "N20 C12 D30 D31", "N21 C13 D32 N22", "C20 D33 N23 C21",
                 "U30 U31 C22 U32", "U33 N30 N31 N32", "N33 S02 S03 C23", "C30 C31 C32 C33",
                 "C00 C01 C02 C03", "E00 E01 E02 E03",
             ),
@@ -568,7 +578,7 @@
                 "K01 K02 K03 F21", "F24 D20 D21 F13", "O00 D13 U10 U11", "F22 D22 U12 F23",
                 "D23 U13 N10 N11", "N12 N13 F30 F31", "F34 U20 U21 U22", "U23 N20 N21 N22",
                 "N23 F32 F33 P30", "D30 D31 D32 D33", "C10 C11 C12 C13", "C20 C21 U30 U31",
-                "C22 C23 U32 U33", "N30 N31 N32 N33", "R20 R21 S00 S01", "S02 S03 R22 C30",
+                "C22 C23 R20 U32", "U33 N30 N31 N32", "N33 R21 S00 S01", "S02 S03 R22 C30",
                 "R10 C31 R23 C32", "R11 C33 R12 C00", "R30 R13 C01 R31", "C02 R32 C03 E10",
                 "R33 E11 E12 E13",
             ),
@@ -653,7 +663,7 @@
             pltpu.VMEM((planes + 1, PARTS, rows, tile), BF16),
             dma((14,)), dma((4,)), dma((2, 2)), dma((3,)), dma((3,)), dma((planes - 1,)), dma((planes,)),
             dma, dma, dma((planes, PARTS + 1)), dma, dma((planes, PARTS)), dma, dma((planes, PARTS)),
-            dma, dma((planes + 1, PARTS)),
+            dma, dma((planes + 1, PARTS + 1)),
         ],
         compiler_params=pltpu.CompilerParams(
             collective_id=0, has_side_effects=True, vmem_limit_bytes=48 * 1024 * 1024

time: 74 us -> 73.2 us (0.989)
  Pallas kernels: 73.1 us -> 72.2 us
    pallas_call x1, Pallas kernels: 73.1 us -> 72.2 us  [fused(): pl.pallas_call(functools.partial(fused_kernel, tp_size, planes, per_plane...]
where the time goes in v5:
time: 73.2 us; the launch traced here: 73 us
  Pallas kernels  72.2 us (99%)
  local copies, waits for them, and re-layouts  0.8 us (1%)
    pallas_call x1, Pallas kernels, fused(): pl.pallas_call(functools.partial(fused_kernel, tp_size, planes, per_plane...  72.2 us

profile of v5, /device:TPU:8, one launch (start us, length us, event | category | flops | bytes accessed | tf_op | source)
XLA Modules:
  0.0 73.0 jit_solution(2191563480199227978)
XLA Ops:
  0.0 72.2 %shard_map.136 = bf16[128,2048]{1,0:T(8,128)(2,1)S(1)} custom-call(bf16[256,512]{1,0:T(8,128)(2,1)} %inner_hbm.1, bf16[256,512]{1,0:T(8,128)(2,1)} %values_hbm.1, s32[2,128]{1,0:T(2,128)} %bitcast.6, f32[2,128]{1,0:T(2,128)} %bitcast.7, f32[1,128]{1,0:T(1,128)} %bitcast.9, s32[1,256]{1,0:T(1,128)} %bitcast.8, f32[3,512]{1,0:T(4,128)} %taps_hbm.1, ...), custom_call_target="tpu_custom_call" | custom-call | tf_op jit(solution)/shard_map/pallas_call | solution.py:627
  72.2 0.8 %copy.16 = bf16[128,2048]{1,0:T(8,128)(2,1)} copy(bf16[128,2048]{1,0:T(8,128)(2,1)S(1)} %shard_map.136) | data formatting | bytes 1048576
